TPU v7x, 32 devices: a whole 2x2x4 slice. The times are simulated.
32 devices in a mesh: sp: 8 (over z, x), tp: 4 (over y, core).
Axes of the slice: x: 2, y: 2, z: 4, core: 2. Of those that a mesh axis runs over, the one named last changes fastest.
Arguments:
- stream_in: bfloat16 [2048, 2048], P(('sp', 'tp')), may hold values from -6 to 6
- pre_gate: bfloat16 [2048, 1024], P('sp', 'tp'), may hold values from -6 to 6
- value_in: bfloat16 [2048, 1024], P('sp', 'tp'), may hold values from -6 to 6
- post_gate: bfloat16 [2048, 1024], P('sp', 'tp'), may hold values from -6 to 6
- conv_taps: bfloat16 [3, 1024], P(None, 'tp'), may hold values from -3 to 3
- out_weight: bfloat16 [1024, 2048], P('tp'), may hold values from -0.1875 to 0.1875
- route_ids: int32 [2048, 4], P('sp'), may hold values from 0 to 7, all different within a row; in each aligned block of 64 rows (0 to 63, 64 to 127, ...) at most 64 rows name the same one
- route_weight: float32 [2048, 4], P('sp'), may hold values from 0.1 to 1
- ffn_gain: bfloat16 [2048], replicated, may hold values from 0.099609375 to 1.8984375
- post_gain: bfloat16 [2048], replicated, may hold values from 0.099609375 to 1.8984375
- gate_proj: bfloat16 [8, 2048, 2048], P('sp', None, 'tp'), may hold values from -0.39648438 to 0.39648438
- up_proj: bfloat16 [8, 2048, 2048], P('sp', None, 'tp'), may hold values from -0.39648438 to 0.39648438
- down_proj: bfloat16 [8, 2048, 2048], P('sp', None, 'tp'), may hold values from -0.125 to 0.125
Outputs:
- layer_out: bfloat16 [2048, 2048], P(('sp', 'tp'))
Inputs may be any that keep to these rules, and one draw needn't show every extreme that they name: `route_ids`: in each aligned block of 64 positions, a row names 4 different experts and no expert is named by more than 64 rows; in every draw some expert reaches 64 in some block.
All inputs are finite; a program needn't handle non-finite values.
Results may differ from a plain program's by a relative error of at most 0.014.
Values may be sent and summed in bfloat16 or wider, within the bound.
A program may use at most 64 MiB of HBM per device.

v0:
```python
import functools

import jax
import jax.numpy as jnp
from jax import lax
from jax.experimental import pallas as pl
from jax.experimental.pallas import tpu as pltpu
from jax.sharding import PartitionSpec as P

clamp_limit = 7.0
sigmoid_scale = 1.702
epsilon = 1e-06


def passed_along(array, axis, by):
    count = lax.axis_size(axis)
    pairs = [(i, i + by) for i in range(count) if 0 <= i + by < count]
    return lax.ppermute(array, axis, pairs)


def clamped_units(gate_pre, up_pre):
    gate_cut = jnp.minimum(gate_pre, clamp_limit)
    up_cut = jnp.clip(up_pre, -clamp_limit, clamp_limit)
    return (up_cut + 1.0) * (gate_cut * jax.nn.sigmoid(sigmoid_scale * gate_cut))


def scaled_norm(values, gain):
    return (
        values
        * lax.rsqrt(jnp.mean(values * values, axis=-1, keepdims=True) + epsilon)
        * gain.astype(jnp.float32)
    )


def block_ranks(route_rows, experts, block_rows):
    flattened = route_rows.reshape(-1)
    entries = flattened.shape[0]
    span_width = block_rows * route_rows.shape[1]
    onehot = (flattened[:, None] == jnp.arange(experts, dtype=jnp.int32)[None, :]).astype(jnp.int32)
    blocked = onehot.reshape(entries // span_width, span_width, experts)
    before = jnp.cumsum(blocked, axis=1) - blocked
    return jnp.sum(before * blocked, axis=2).reshape(route_rows.shape)


def slot_picker(slot_index, table_size):
    matches = slot_index[None, :, :] == jnp.arange(table_size, dtype=jnp.int32)[:, None, None]
    return jnp.any(matches, axis=2).astype(jnp.bfloat16)


LANES = 128


def table_pick(table, first, second):
    value = jnp.int32(0)
    for i, row in enumerate(table):
        for j, entry in enumerate(row):
            if entry:
                value = value + jnp.where((first == i) & (second == j), entry, 0)
    return value


def layer_kernel(
    sp_count,
    stream_ref,
    pre_ref,
    value_ref,
    post_ref,
    taps_ref,
    ids_ref,
    weight_ref,
    gain_ref,
    post_gain_ref,
    out_hbm,
    gate_hbm,
    up_hbm,
    down_hbm,
    result_ref,
    out_w,
    gate_w,
    up_w,
    down_w,
    tail,
    rim,
    padded,
    mixed,
    pair_send,
    pair_in,
    own_sum,
    y_send,
    y_in,
    resid,
    tokens,
    hidden,
    part,
    chain_in,
    x_in,
    final,
    columns,
    load_sem,
    rim_sem,
    proj_sem,
    y_sem,
    tok_send,
    tok_recv,
    hid_send,
    hid_recv,
    chain_send,
    chain_recv,
    x_send,
    x_recv,
    fin_send,
    fin_recv,
):
    f32, bf16 = jnp.float32, jnp.bfloat16
    heights = sp_count // 2
    sp = lax.axis_index("sp")
    tp = lax.axis_index("tp")
    z, x = lax.div(sp, 2), lax.rem(sp, 2)
    y, c = lax.div(tp, 2), lax.rem(tp, 2)
    across, sibling = sp + 1 - 2 * x, tp + 1 - 2 * c
    opposite = lax.rem(tp + 2, 4)
    rows, width = stream_ref.shape
    seq = 4 * rows
    half = 2 * rows
    units = gate_w.shape[1]

    def at(sp_to, tp_to):
        return {"sp": sp_to, "tp": tp_to}

    def remote(source, target, send, receive, device):
        return pltpu.make_async_remote_copy(
            src_ref=source,
            dst_ref=target,
            send_sem=send,
            recv_sem=receive,
            device_id=device,
            device_id_type=pl.DeviceIdType.MESH,
        )

    loads = [
        pltpu.make_async_copy(source, target, load_sem.at[i])
        for i, (source, target) in enumerate(
            ((out_hbm, out_w), (gate_hbm.at[0], gate_w), (up_hbm.at[0], up_w), (down_hbm.at[0], down_w))
        )
    ]
    for load in loads:
        load.start()

    barrier = pltpu.get_barrier_semaphore()
    partners = [at(lax.rem(sp + by, sp_count), tp) for by in (1, 2, sp_count - 1, sp_count - 2)]
    partners += [at(across, tp), at(sp, sibling), at(sp, opposite), at(sp, 3 - tp)]
    for partner in partners:
        pl.semaphore_signal(barrier, inc=1, device_id=partner, device_id_type=pl.DeviceIdType.MESH)
    pl.semaphore_wait(barrier, len(partners))

    gated = (pre_ref[...].astype(f32) * value_ref[...].astype(f32)).astype(bf16)
    tail[...] = gated[seq - 16 :]
    rim_copy = remote(tail, rim, rim_sem.at[0], rim_sem.at[1], at(lax.rem(sp + 1, sp_count), tp))
    rim_copy.start()
    padded[8:, :] = gated.astype(f32)
    lane = lax.broadcasted_iota(jnp.int32, (rows, LANES), 1)
    row = lax.broadcasted_iota(jnp.int32, (rows, seq), 0)
    picked = (lax.broadcasted_iota(jnp.int32, (rows, seq), 1) == row + tp * rows).astype(bf16)

    def own_columns(values):
        return lax.dot_general(picked, values, (((1,), (1,)), ((), ())), preferred_element_type=f32)

    top_count = ids_ref.shape[0]
    weights = weight_ref[...]
    high = weights.astype(bf16)
    low = own_columns((weights - high.astype(f32)).astype(bf16))
    high = own_columns(high)
    ids = own_columns(ids_ref[...].astype(f32).astype(bf16)).astype(jnp.int32)
    spread = jnp.zeros((rows, LANES), f32)
    for k in range(top_count):
        spread = spread + jnp.where(lane == ids[:, k : k + 1], high[:, k : k + 1], 0.0)
        spread = spread + jnp.where(lane == ids[:, k : k + 1] + sp_count, low[:, k : k + 1], 0.0)
    own_row = pl.multiple_of(c * half + y * rows, rows)
    tokens[sp, pl.ds(own_row, rows), width:] = spread.astype(bf16)
    rim_copy.wait()
    padded[:8, :] = jnp.where(sp == 0, 0.0, rim[...].astype(f32)[8:])
    tap_count = taps_ref.shape[0]
    taps = taps_ref[...].astype(f32)
    convolved = jnp.zeros((seq, padded.shape[1]), f32)
    for k in range(tap_count):
        first = 8 - tap_count + 1 + k
        convolved = convolved + taps[k : k + 1, :] * padded[first : first + seq, :]
    mixed[...] = (post_ref[...].astype(f32) * convolved).astype(bf16)
    loads[0].wait()

    def rows_of(core):
        return jnp.concatenate(
            [mixed[pl.ds(pl.multiple_of(yy * half + core * rows, rows), rows), :] for yy in range(2)], 0
        )

    pair_send[...] = jnp.dot(rows_of(1 - c), out_w[...], preferred_element_type=f32).astype(bf16)
    pair_copy = remote(pair_send, pair_in, proj_sem.at[0], proj_sem.at[1], at(sp, sibling))
    pair_copy.start()
    own_sum[...] = jnp.dot(rows_of(c), out_w[...], preferred_element_type=f32)
    pair_copy.wait()
    far = pl.ds(pl.multiple_of((1 - y) * rows, rows), rows)
    near = pl.ds(pl.multiple_of(y * rows, rows), rows)
    y_send[...] = (own_sum[far, :] + pair_in[far, :].astype(f32)).astype(bf16)
    y_copy = remote(y_send, y_in, proj_sem.at[2], proj_sem.at[3], at(sp, opposite))
    y_copy.start()
    own_sum[near, :] = own_sum[near, :] + pair_in[near, :].astype(f32)
    y_copy.wait()
    residual = (stream_ref[...].astype(f32) + (own_sum[near, :] + y_in[...].astype(f32))).astype(bf16)
    resid[...] = residual
    tokens[sp, pl.ds(own_row, rows), :width] = scaled_norm(residual.astype(f32), gain_ref[...].reshape(1, width)).astype(bf16)

    def block_of(group, slot):
        return tokens.at[group, pl.ds(pl.multiple_of(slot * rows, rows), rows), :]

    own_block = block_of(sp, 2 * c + y)
    block_copy = remote(own_block, own_block, y_sem.at[0], tok_recv.at[sp, 2 * c + y], at(sp, opposite))

    def forward(way, group, yy):
        device = (
            at(lax.rem(sp + 2, sp_count), tp),
            at(lax.rem(sp + sp_count - 2, sp_count), tp),
            at(across, tp),
            at(sp, sibling),
        )[way]
        block = block_of(group, 2 * c + yy)
        return remote(block, block, tok_send.at[way, group, yy], tok_recv.at[group, 2 * c + yy], device)

    def arrival(group, slot):
        block = block_of(group, slot)
        return remote(block, block, y_sem.at[0], tok_recv.at[group, slot], at(sp, sibling))

    def share(way, group):
        whose = tp if way < 2 else opposite
        block = hidden.at[group, whose]
        return remote(
            block, block, hid_send.at[way, group], hid_recv.at[group, whose], at(sp, sibling if way else opposite)
        )

    def shared(group, whose):
        block = hidden.at[group, whose]
        return remote(block, block, hid_send.at[0, group], hid_recv.at[group, whose], at(sp, sibling))

    near_first = [sorted(range(heights), key=lambda other: abs(other - i)) for i in range(heights)]
    home_order = [
        sorted(
            range(heights),
            key=lambda other: (other == i, heights - 1 - i if other < i else i, abs(other - i)),
        )
        for i in range(heights)
    ]

    def group_at(tick):
        height = table_pick(near_first, z, lax.div(tick, 2))
        own_x = lax.rem(tick, 2) == 0
        return height, 2 * height + jnp.where(own_x, x, 1 - x)

    def piece_of(part_number):
        return pl.ds(part_number * rows, rows)

    def over_x(height, h):
        return remote(
            part.at[2 * height + 1 - x, piece_of(h), :],
            x_in.at[height, piece_of(h), :],
            x_send.at[height, h],
            x_recv.at[height, h],
            at(across, tp),
        )

    def homeward(height, down_side, h):
        device = at(lax.rem(sp + (sp_count - 2, 2)[down_side], sp_count), tp)
        return remote(
            part.at[2 * height + x, piece_of(h), :],
            chain_in.at[down_side, height, piece_of(h), :],
            chain_send.at[height, h],
            chain_recv.at[down_side, height, h],
            device,
        )

    last = heights - 1

    def own_side(step):
        height = table_pick(near_first, z, lax.div(step, 2))
        return height, jnp.where(lax.rem(step, 2) == 0, y, 1 - y)

    def take_own(height, yy):
        group = 2 * height + x
        arrival(group, 2 * c + yy).wait_recv()

        @pl.when((height <= z) & (z < last))
        def _():
            forward(0, group, yy).start()

        @pl.when((height >= z) & (z > 0))
        def _():
            forward(1, group, yy).start()

        forward(3, group, yy).start()

    def send_across(step):
        height, yy = own_side(step)
        forward(2, 2 * height + x, yy).start()

    def take_across(step):
        height, yy = own_side(step)
        group = 2 * height + 1 - x
        arrival(group, 2 * c + yy).wait_recv()
        forward(3, group, yy).start()

    def gated_units(tick):
        _, group = group_at(tick)
        for yy in range(2):
            arrival(group, 2 * (1 - c) + yy).wait_recv()
        inputs = tokens[group, :, :width]
        tile = min(256, units)
        for start in range(0, units, tile):
            gate_pre = jnp.dot(inputs, gate_w[:, start : start + tile], preferred_element_type=f32)
            up_pre = jnp.dot(inputs, up_w[:, start : start + tile], preferred_element_type=f32)
            hidden[group, tp, :, start : start + tile] = clamped_units(gate_pre, up_pre).astype(bf16)
        share(0, group).start()
        share(1, group).start()

    def relay_units(tick):
        _, group = group_at(tick)
        shared(group, opposite).wait_recv()
        share(2, group).start()

    def project_down(tick):
        height, group = group_at(tick)
        shared(group, sibling).wait_recv()
        shared(group, 3 - tp).wait_recv()
        total = jnp.dot(hidden[group, 0], down_w[:units, :], preferred_element_type=f32)
        for k in range(1, 4):
            total = total + jnp.dot(
                hidden[group, k], down_w[k * units : (k + 1) * units, :], preferred_element_type=f32
            )
        lanes = lax.broadcasted_iota(jnp.int32, (seq, LANES), 1)
        mine = (lanes == sp) | (lanes == sp + sp_count)
        scale = jnp.sum(jnp.where(mine, tokens[group, :, width:].astype(f32), 0.0), axis=1, keepdims=True)
        part[group] = (total.astype(bf16).astype(f32) * scale).astype(bf16)

        @pl.when((lax.rem(tick, 2) == 1) & (tick > 1))
        def _():
            for h in range(4):
                over_x(height, h).start()

    block_copy.start()
    for way, there in ((0, z < last), (1, z > 0)):

        @pl.when(there)
        def _():
            forward(way, sp, y).start()

    forward(2, sp, y).start()
    forward(3, sp, y).start()
    take_own(z, 1 - y)
    send_across(jnp.int32(1))
    for load in loads[1:]:
        load.wait()

    def take_step(step, yy):
        distance = lax.div(step, 2) + 1

        @pl.when(z >= distance)
        def _():
            take_own(z - distance, yy)

        @pl.when(z + distance <= last)
        def _():
            take_own(z + distance, yy)

        send_across(step + 2)

    gated_units(jnp.int32(0))

    def round_body(j, carry):
        early, late = 2 * j, 2 * j + 1

        @pl.when(j < last)
        def _():
            take_step(early, y)

        take_across(early)

        @pl.when(j >= 1)
        def _():
            relay_units(early - 1)
            project_down(early - 2)

        @pl.when(j < last)
        def _():
            take_step(late, 1 - y)

        take_across(late)
        gated_units(late)

        @pl.when(j < last)
        def _():
            gated_units(late + 1)

        relay_units(early)

        @pl.when(j >= 1)
        def _():
            project_down(early - 1)

        return carry

    lax.fori_loop(0, heights, round_body, 0)

    def f32_half(ref, index, h):
        return ref[index, piece_of(h), :].astype(f32)

    def go_home(item):
        height = table_pick(home_order, z, item)
        group = 2 * height + x
        from_above = (height < z) & (z < last)
        from_below = (height > z) & (z > 0)
        for h in range(4):
            over_x(height, h).wait_recv()

            @pl.when(jnp.logical_not(from_above | from_below))
            def _():
                part[group, piece_of(h), :] = (f32_half(part, group, h) + f32_half(x_in, height, h)).astype(bf16)

            for down_side, comes in enumerate((from_above, from_below)):

                @pl.when(comes)
                def _():
                    homeward(height, down_side, h).wait_recv()
                    total = f32_half(part, group, h) + f32_half(x_in, height, h)
                    total = total + chain_in[down_side, height, piece_of(h), :].astype(f32)
                    part[group, piece_of(h), :] = total.astype(bf16)

            @pl.when(height < z)
            def _():
                homeward(height, 0, h).start()

            @pl.when(height > z)
            def _():
                homeward(height, 1, h).start()

    at_end = (z == 0) | (z == last)
    early_items = min(2, last)

    def go_early(item):
        @pl.when(at_end)
        def _():
            go_home(jnp.int32(item))

    go_early(0)
    relay_units(sp_count - 1)
    project_down(sp_count - 2)
    if early_items > 1:
        go_early(1)
    project_down(sp_count - 1)
    for h in range(4):
        over_x(z, h).start()

    def home_body(item, carry):
        @pl.when(jnp.logical_not(at_end) | (item >= early_items))
        def _():
            go_home(item)

        return carry

    lax.fori_loop(0, last, home_body, 0)

    def hand_over(h, yy):
        return remote(
            final.at[pl.ds(h * half + yy * rows, rows), :],
            columns.at[tp],
            fin_send.at[2 * h + yy],
            fin_recv.at[tp],
            at(sp, 2 * yy + h),
        )

    for h in range(4):
        over_x(z, h).wait_recv()
        part[sp, piece_of(h), :] = (f32_half(part, sp, h) + f32_half(x_in, z, h)).astype(bf16)
        for down_side, comes in enumerate((z < last, z > 0)):

            @pl.when(comes)
            def _():
                homeward(z, down_side, h).wait_recv()
                part[sp, piece_of(h), :] = (
                    f32_half(part, sp, h) + chain_in[down_side, z, piece_of(h), :].astype(f32)
                ).astype(bf16)

        final[piece_of(h), :] = part[sp, piece_of(h), :]
        core, yy = h // 2, h % 2

        @pl.when(tp != 2 * yy + core)
        def _():
            hand_over(core, yy).start()

    columns[tp] = final[pl.ds(own_row, rows), :]
    for step in (1, 2, 3):
        whose = lax.rem(tp + step, 4)
        remote(
            final.at[pl.ds(0, rows), :], columns.at[whose], fin_send.at[0], fin_recv.at[whose], at(sp, sibling)
        ).wait_recv()
    combined = jnp.concatenate([columns[k] for k in range(4)], 1).astype(f32)
    result_ref[...] = (
        resid[...].astype(f32) + scaled_norm(combined, post_gain_ref[...].reshape(1, width))
    ).astype(bf16)

    block_copy.wait_send()
    for h in range(2):
        for yy in range(2):

            @pl.when(tp != 2 * yy + h)
            def _():
                hand_over(h, yy).wait_send()

    def drain(group, carry):
        height = lax.div(group, 2)

        for yy in range(2):

            @pl.when(lax.rem(group, 2) == x)
            def _():
                @pl.when((height <= z) & (z < last))
                def _():
                    forward(0, group, yy).wait_send()

                @pl.when((height >= z) & (z > 0))
                def _():
                    forward(1, group, yy).wait_send()

                forward(2, group, yy).wait_send()

            forward(3, group, yy).wait_send()
        for way in range(3):
            share(way, group).wait_send()

        @pl.when(lax.rem(group, 2) == 0)
        def _():
            for h in range(4):
                over_x(height, h).wait_send()

                @pl.when(height != z)
                def _():
                    homeward(height, 0, h).wait_send()

        return carry

    lax.fori_loop(0, sp_count, drain, 0)


def dense_layer(
    stream_in,
    pre_gate,
    value_in,
    post_gate,
    conv_taps,
    out_weight,
    route_ids,
    route_weight,
    ffn_gain,
    post_gain,
    gate_proj,
    up_proj,
    down_proj,
):
    sp_count = lax.axis_size("sp")
    rows, width = stream_in.shape
    seq, channels = pre_gate.shape
    units = gate_proj.shape[2]
    cols = down_proj.shape[2]
    bf16, f32 = jnp.bfloat16, jnp.float32
    dma = pltpu.SemaphoreType.DMA
    scratch = [
        pltpu.VMEM(out_weight.shape, bf16),
        pltpu.VMEM(gate_proj.shape[1:], bf16),
        pltpu.VMEM(up_proj.shape[1:], bf16),
        pltpu.VMEM(down_proj.shape[1:], bf16),
        pltpu.VMEM((16, channels), bf16),
        pltpu.VMEM((16, channels), bf16),
        pltpu.VMEM((seq + 8, channels), f32),
        pltpu.VMEM((seq, channels), bf16),
        pltpu.VMEM((2 * rows, width), bf16),
        pltpu.VMEM((2 * rows, width), bf16),
        pltpu.VMEM((2 * rows, width), f32),
        pltpu.VMEM((rows, width), bf16),
        pltpu.VMEM((rows, width), bf16),
        pltpu.VMEM((rows, width), bf16),
        pltpu.VMEM((sp_count, seq, width + LANES), bf16),
        pltpu.VMEM((sp_count, 4, seq, units), bf16),
        pltpu.VMEM((sp_count, seq, cols), bf16),
        pltpu.VMEM((2, sp_count // 2, seq, cols), bf16),
        pltpu.VMEM((sp_count // 2, seq, cols), bf16),
        pltpu.VMEM((seq, cols), bf16),
        pltpu.VMEM((4, rows, cols), bf16),
        dma((4,)),
        dma((2,)),
        dma((4,)),
        dma((1,)),
        dma((4, sp_count, 2)),
        dma((sp_count, 4)),
        dma((3, sp_count)),
        dma((sp_count, 4)),
        dma((sp_count // 2, 4)),
        dma((2, sp_count // 2, 4)),
        dma((sp_count // 2, 4)),
        dma((sp_count // 2, 4)),
        dma((4,)),
        dma((4,)),
    ]
    vmem = pl.BlockSpec(memory_space=pltpu.VMEM)
    anywhere = pl.BlockSpec(memory_space=pl.ANY)
    return pl.pallas_call(
        functools.partial(layer_kernel, sp_count),
        out_shape=jax.ShapeDtypeStruct((rows, width), bf16),
        in_specs=[vmem] * 9 + [anywhere] * 4,
        out_specs=vmem,
        scratch_shapes=scratch,
        compiler_params=pltpu.CompilerParams(
            collective_id=0, has_side_effects=True, vmem_limit_bytes=58 * 1024 * 1024
        ),
    )(
        stream_in,
        pre_gate,
        value_in,
        post_gate,
        conv_taps,
        route_ids.T,
        route_weight.T,
        ffn_gain,
        post_gain,
        out_weight,
        gate_proj,
        up_proj,
        down_proj,
    )


def local(
    stream_in,
    pre_gate,
    value_in,
    post_gate,
    conv_taps,
    out_weight,
    route_ids,
    route_weight,
    ffn_gain,
    post_gain,
    gate_proj,
    up_proj,
    down_proj,
):
    sp_count = lax.axis_size("sp")
    tp_count = lax.axis_size("tp")
    seq_rows = pre_gate.shape[0]
    own_rows = seq_rows // tp_count
    top_count = route_ids.shape[1]
    slots_each = 2 * own_rows * top_count // sp_count
    if tp_count == 4 and sp_count % 2 == 0 and slots_each >= own_rows:
        return dense_layer(
            stream_in, pre_gate, value_in, post_gate, conv_taps, out_weight, route_ids, route_weight,
            ffn_gain, post_gain, gate_proj, up_proj, down_proj,
        )
    tap_count = conv_taps.shape[0]
    gated_input = (pre_gate.astype(jnp.float32) * value_in.astype(jnp.float32)).astype(jnp.bfloat16)
    rim_rows = passed_along(gated_input[seq_rows - tap_count + 1 :], "sp", 1)
    padded = jnp.concatenate([rim_rows, gated_input], 0).astype(jnp.float32)
    convolved = jnp.zeros(gated_input.shape, jnp.float32)
    for tap_index in range(tap_count):
        convolved = (
            convolved
            + conv_taps[tap_index].astype(jnp.float32)[None, :]
            * padded[tap_index : tap_index + seq_rows]
        )
    mixer_out = (post_gate.astype(jnp.float32) * convolved).astype(jnp.bfloat16)
    weight_rows = mixer_out
    projected = lax.psum_scatter(
        jnp.dot(weight_rows, out_weight, preferred_element_type=jnp.float32),
        "tp",
        scatter_dimension=0,
        tiled=True,
    )
    residual = (stream_in.astype(jnp.float32) + projected).astype(jnp.bfloat16)
    normed = scaled_norm(residual.astype(jnp.float32), ffn_gain).astype(jnp.bfloat16)
    slot_rank = block_ranks(route_ids, sp_count, own_rows)
    block_of = (jnp.arange(seq_rows, dtype=jnp.int32) // own_rows)[:, None]
    tp_index = lax.axis_index("tp")
    own_ids = lax.dynamic_slice_in_dim(route_ids, tp_index * own_rows, own_rows, 0)
    own_rank = lax.dynamic_slice_in_dim(slot_rank, tp_index * own_rows, own_rows, 0)
    own_slot = own_ids * slots_each + own_rank
    picker = slot_picker(own_slot, sp_count * slots_each)
    outgoing = jnp.dot(picker, normed, preferred_element_type=jnp.float32).astype(jnp.bfloat16)
    arrived = lax.all_to_all(outgoing, "sp", split_axis=0, concat_axis=0, tiled=True)
    portion = lax.all_gather(arrived, "tp", axis=0, tiled=True)
    gate_pre = jnp.dot(portion, gate_proj[0], preferred_element_type=jnp.float32)
    up_pre = jnp.dot(portion, up_proj[0], preferred_element_type=jnp.float32)
    hidden = clamped_units(gate_pre, up_pre).astype(jnp.bfloat16)
    weight_rows = down_proj[0]
    column_out = jnp.dot(
        lax.all_gather(hidden, "tp", axis=1, tiled=True),
        weight_rows,
        preferred_element_type=jnp.float32,
    ).astype(jnp.bfloat16)
    column_width = column_out.shape[1]
    returned = lax.all_to_all(
        column_out.reshape(tp_count, sp_count, slots_each, column_width),
        "sp",
        split_axis=1,
        concat_axis=1,
        tiled=True,
    )
    home_index = (block_of * sp_count + route_ids) * slots_each + slot_rank
    gathered_out = jnp.take(returned.reshape(-1, column_width), home_index.reshape(-1), axis=0)
    gathered_out = gathered_out.astype(jnp.float32).reshape(seq_rows, top_count, column_width)
    combined_cols = jnp.sum(gathered_out * route_weight[:, :, None], axis=1).astype(jnp.bfloat16)
    combined = lax.all_to_all(combined_cols, "tp", split_axis=0, concat_axis=1, tiled=True)
    layer_out = residual.astype(jnp.float32) + scaled_norm(combined.astype(jnp.float32), post_gain)
    return layer_out.astype(jnp.bfloat16)


def solution(mesh):
    placed = (
        P(("sp", "tp"), None),
        P("sp", "tp"),
        P("sp", "tp"),
        P("sp", "tp"),
        P(None, "tp"),
        P("tp", None),
        P("sp", None),
        P("sp", None),
        P(),
        P(),
        P("sp", None, "tp"),
        P("sp", None, "tp"),
        P("sp", None, "tp"),
    )
    return jax.shard_map(
        local, mesh=mesh, in_specs=placed, out_specs=P(("sp", "tp"), None), check_vma=False
    )
```

profile of v0, /device:TPU:1, one launch (start us, length us, event | category | flops | bytes accessed | tf_op | source)
XLA Modules:
  0.0 110.3 jit_solution(8662526839238270879)
XLA Ops:
  0.0 108.7 %shard_map.127 = bf16[64,2048]{1,0:T(8,128)(2,1)} custom-call(bf16[64,2048]{1,0:T(8,128)(2,1)} %stream_ref.1, bf16[256,256]{1,0:T(8,128)(2,1)} %pre_ref.1, bf16[256,256]{1,0:T(8,128)(2,1)} %value_ref.1, bf16[256,256]{1,0:T(8,128)(2,1)} %post_ref.1, bf16[3,256]{1,0:T(4,128)(2,1)} %taps_ref.1, s32[4,256]{1,0:T(4,128)} %bitcast.2, f32[4,256]{1,0:T(4,128)} %bitcast.3, ...), custom_call_target="tpu_custom_call" | custom-call | tf_op jit(solution)/shard_map/pallas_call | solution.py:611
  108.7 1.7 %copy.15 = bf16[64,2048]{1,0:T(8,128)(2,1)} copy(bf16[64,2048]{1,0:T(8,128)(2,1)} %shard_map.127) | data formatting | bytes 524288
where the time goes:
time: 111 us; the launch traced here: 110 us
  Pallas kernels  109 us (98%)
  local copies, waits for them, and re-layouts  1.67 us (2%)
    pallas_call x1, Pallas kernels, dense_layer(): pl.pallas_call(functools.partial(layer_kernel, sp_count), out_shape=jax.S...  109 us

commit v1 on v0

v1 whole, which is shorter than its diff:
```python
import functools

import jax
import jax.numpy as jnp
from jax import lax
from jax.experimental import pallas as pl
from jax.experimental.pallas import tpu as pltpu
from jax.sharding import PartitionSpec as P

clamp_limit = 7.0
sigmoid_scale = 1.702
epsilon = 1e-06


def passed_along(array, axis, by):
    count = lax.axis_size(axis)
    pairs = [(i, i + by) for i in range(count) if 0 <= i + by < count]
    return lax.ppermute(array, axis, pairs)


def clamped_units(gate_pre, up_pre):
    gate_cut = jnp.minimum(gate_pre, clamp_limit)
    up_cut = jnp.clip(up_pre, -clamp_limit, clamp_limit)
    return (up_cut + 1.0) * (gate_cut * jax.nn.sigmoid(sigmoid_scale * gate_cut))


def scaled_norm(values, gain):
    return (
        values
        * lax.rsqrt(jnp.mean(values * values, axis=-1, keepdims=True) + epsilon)
        * gain.astype(jnp.float32)
    )


def block_ranks(route_rows, experts, block_rows):
    flattened = route_rows.reshape(-1)
    entries = flattened.shape[0]
    span_width = block_rows * route_rows.shape[1]
    onehot = (flattened[:, None] == jnp.arange(experts, dtype=jnp.int32)[None, :]).astype(jnp.int32)
    blocked = onehot.reshape(entries // span_width, span_width, experts)
    before = jnp.cumsum(blocked, axis=1) - blocked
    return jnp.sum(before * blocked, axis=2).reshape(route_rows.shape)


def slot_picker(slot_index, table_size):
    matches = slot_index[None, :, :] == jnp.arange(table_size, dtype=jnp.int32)[:, None, None]
    return jnp.any(matches, axis=2).astype(jnp.bfloat16)


PIECES = 4
PLANNED_GROUPS = 8
end_plan = (
    32, 33, 4, 8, 10, 5, 96, 11, 35, 6, 16, 7, 34, 18, 98, 19, 43, 9, 17, 97,
    104, 26, 24, 48, 25, 27, 51, 49, 42, 41, 40, 50, 131, 108, 31, 28, 106, 30, 29, 66,
    58, 57, 64, 109, 56, 59, 137, 141, 110, 173, 60, 63, 62, 67, 61, 65, 140, 111, 172, 22,
    38, 23, 102, 143, 129, 39, 21, 20, 36, 15, 175, 142, 105, 55, 37, 174, 13, 12, 99, 53,
    54, 52, 139, 135, 14, 169, 107, 128, 136, 101, 171, 161, 130, 44, 168, 47, 45, 163, 46, 138,
    103, 170, 100, 160, 167, 162, 134, 132, 166, 194, 133, 164, 165, 195, 192, 193,
)
middle_plan = (
    9, 8, 16, 18, 96, 19, 10, 17, 4, 34, 104, 24, 11, 26, 5, 6, 7, 12, 14, 15,
    13, 25, 27, 100, 28, 108, 101, 31, 49, 51, 50, 48, 30, 29, 71, 109, 106, 68, 69, 97,
    33, 70, 58, 47, 46, 141, 140, 44, 45, 23, 32, 22, 20, 21, 103, 137, 133, 59, 56, 105,
    172, 57, 35, 165, 173, 60, 62, 63, 61, 40, 41, 111, 110, 136, 139, 42, 55, 43, 204, 129,
    205, 132, 52, 54, 169, 65, 66, 64, 67, 142, 53, 102, 168, 174, 128, 134, 107, 143, 206, 166,
    38, 197, 175, 135, 207, 171, 98, 167, 198, 37, 39, 36, 160, 138, 203, 161, 99, 199, 164, 170,
    196, 202, 131, 163, 195, 130, 201, 162, 200, 194, 192, 193,
)

def words_of(plan):
    codes = list(plan)
    codes += [255] * (-len(codes) % 4)
    words = [sum(code << (8 * i) for i, code in enumerate(codes[at : at + 4])) for at in range(0, len(codes), 4)]
    return [word - (1 << 32) if word >> 31 else word for word in words]


def pick(at_end, tables, position):
    value = jnp.int32(-1)
    for i, table in enumerate(tables):
        chosen = jnp.int32(-1)
        for j, word in enumerate(table):
            chosen = jnp.where(position == j, word, chosen)
        value = jnp.where(at_end == (i == 0), chosen, value)
    return value


def layer_kernel(
    sp_count,
    stream_ref,
    pre_ref,
    value_ref,
    post_ref,
    taps_ref,
    ids_ref,
    weight_ref,
    gain_ref,
    post_gain_ref,
    out_hbm,
    gate_hbm,
    up_hbm,
    down_hbm,
    result_ref,
    out_w,
    gate_w,
    up_w,
    down_w,
    tail,
    rim,
    padded,
    mixed,
    pair_send,
    pair_in,
    own_sum,
    y_send,
    y_in,
    resid,
    scales,
    tokens,
    hidden,
    part,
    chain_in,
    x_in,
    total,
    final,
    columns,
    load_sem,
    rim_sem,
    pair_sem,
    y_sem,
    y_recv,
    scale_send,
    scale_recv,
    tok_send,
    tok_recv,
    mate_recv,
    hid_send,
    hid_recv,
    chain_send,
    chain_recv,
    x_send,
    x_recv,
    fin_send,
    fin_recv,
):
    f32, bf16 = jnp.float32, jnp.bfloat16
    heights = sp_count // 2
    last = heights - 1
    sp = lax.axis_index("sp")
    tp = lax.axis_index("tp")
    z, x = lax.div(sp, 2), lax.rem(sp, 2)
    y, c = lax.div(tp, 2), lax.rem(tp, 2)
    across, sibling = sp + 1 - 2 * x, tp + 1 - 2 * c
    opposite = lax.rem(tp + 2, 4)
    rows, width = stream_ref.shape
    seq = 4 * rows
    half = 2 * rows
    step = rows // PIECES
    units = gate_w.shape[1]
    at_end = (z == 0) | (z == last)
    toward = jnp.where(2 * z < heights, 1, -1)

    def at(sp_to, tp_to):
        return {"sp": sp_to, "tp": tp_to}

    def remote(source, target, send, receive, device):
        return pltpu.make_async_remote_copy(
            src_ref=source,
            dst_ref=target,
            send_sem=send,
            recv_sem=receive,
            device_id=device,
            device_id_type=pl.DeviceIdType.MESH,
        )

    loads = [
        pltpu.make_async_copy(source, target, load_sem.at[i])
        for i, (source, target) in enumerate(
            ((out_hbm, out_w), (gate_hbm.at[0], gate_w), (up_hbm.at[0], up_w), (down_hbm.at[0], down_w))
        )
    ]
    for load in loads:
        load.start()

    barrier = pltpu.get_barrier_semaphore()

    def greet(partner):
        pl.semaphore_signal(barrier, inc=1, device_id=partner, device_id_type=pl.DeviceIdType.MESH)

    for partner in (at(across, tp), at(sp, sibling), at(sp, opposite), at(sp, 3 - tp)):
        greet(partner)
    met = jnp.int32(4)
    for there, by in ((sp < sp_count - 1, 1), (sp > 0, -1), (z < last, 2), (z > 0, -2)):

        @pl.when(there)
        def _():
            greet(at(sp + by, tp))

        met = met + jnp.where(there, 1, 0)
    pl.semaphore_wait(barrier, met)

    gated = (pre_ref[...].astype(f32) * value_ref[...].astype(f32)).astype(bf16)
    tail[...] = gated[seq - 16 :]
    rim_copy = remote(tail, rim, rim_sem.at[0], rim_sem.at[1], at(sp + 1, tp))

    @pl.when(sp < sp_count - 1)
    def _():
        rim_copy.start()

    expert = lax.broadcasted_iota(jnp.int32, (sp_count, seq), 0)
    spread = jnp.zeros((sp_count, seq), f32)
    for k in range(ids_ref.shape[0]):
        spread = spread + jnp.where(expert == ids_ref[k : k + 1, :], weight_ref[k : k + 1, :], 0.0)
    scales[sp] = spread

    routes = (
        lambda group: (lax.div(group, 2) <= z) & (z < last),
        lambda group: (lax.div(group, 2) >= z) & (z > 0),
    )
    devices = (at(sp + 2, tp), at(sp - 2, tp), at(across, tp), at(sp, sibling), at(sp, opposite))

    def scale_copy(way, group):
        return remote(scales.at[group], scales.at[group], scale_send.at[way, group], scale_recv.at[group], devices[way])

    def send_scales(group):
        for way in range(2):

            @pl.when(routes[way](group))
            def _():
                scale_copy(way, group).start()

        scale_copy(2, group).start()

    send_scales(sp)
    padded[8:, :] = gated.astype(f32)

    @pl.when(sp == 0)
    def _():
        padded[:8, :] = jnp.zeros((8, padded.shape[1]), f32)

    @pl.when(sp > 0)
    def _():
        rim_copy.wait_recv()
        padded[:8, :] = rim[...].astype(f32)[8:]

    tap_count = taps_ref.shape[0]
    taps = taps_ref[...].astype(f32)
    convolved = jnp.zeros((seq, padded.shape[1]), f32)
    for k in range(tap_count):
        first = 8 - tap_count + 1 + k
        convolved = convolved + taps[k : k + 1, :] * padded[first : first + seq, :]
    mixed[...] = (post_ref[...].astype(f32) * convolved).astype(bf16)
    loads[0].wait()

    def rows_of(core):
        return jnp.concatenate(
            [mixed[pl.ds(pl.multiple_of(yy * half + core * rows, rows), rows), :] for yy in range(2)], 0
        )

    pair_send[...] = jnp.dot(rows_of(1 - c), out_w[...], preferred_element_type=f32).astype(bf16)
    pair_copy = remote(pair_send, pair_in, pair_sem.at[0], pair_sem.at[1], at(sp, sibling))
    pair_copy.start()
    own_sum[...] = jnp.dot(rows_of(c), out_w[...], preferred_element_type=f32)
    pair_copy.wait()
    far = pl.ds(pl.multiple_of((1 - y) * rows, rows), rows)
    near = pl.ds(pl.multiple_of(y * rows, rows), rows)
    y_send[...] = (own_sum[far, :] + pair_in[far, :].astype(f32)).astype(bf16)

    def y_copy(p):
        piece = pl.ds(p * step, step)
        return remote(y_send.at[piece, :], y_in.at[piece, :], y_sem.at[0], y_recv.at[p], at(sp, opposite))

    for p in range(PIECES):
        y_copy(p).start()
    own_sum[near, :] = own_sum[near, :] + pair_in[near, :].astype(f32)

    def height_of(relative):
        inner = jnp.where(relative == 0, 0, jnp.where(relative == 1, -1, relative - 1))
        return z + toward * jnp.where(at_end, relative, inner)

    def wait_scales(group):
        scale_copy(2, group).wait_recv()

    def take_scales(relative, carry):
        group = 2 * height_of(relative) + x
        wait_scales(group)
        send_scales(group)
        return carry

    lax.fori_loop(1, heights, take_scales, 0)

    def take_scales_across(height, carry):
        wait_scales(2 * height + 1 - x)
        return carry

    lax.fori_loop(0, heights, take_scales_across, 0)

    def piece_of(group, yy, p):
        return tokens.at[group, pl.ds(pl.multiple_of((2 * yy + c) * rows + p * step, step), step), :]

    def block_of(group, yy, core):
        return tokens.at[group, pl.ds(pl.multiple_of((2 * yy + core) * rows, rows), rows), :]

    def pass_on(way, group, yy, p):
        piece = piece_of(group, yy, p)
        receive = mate_recv.at[group, yy] if way == 3 else tok_recv.at[group, yy, p]
        return remote(piece, piece, tok_send.at[way, group, yy], receive, devices[way])

    def sent(way, group, yy):
        block = block_of(group, yy, c)
        return remote(block, block, tok_send.at[way, group, yy], mate_recv.at[group, yy], devices[way])

    def along_z(group, yy, p):
        for way in range(2):

            @pl.when(routes[way](group))
            def _():
                pass_on(way, group, yy, p).start()

    for p in range(PIECES):
        y_copy(p).wait_recv()
        piece = pl.ds(p * step, step)
        own = pl.ds(pl.multiple_of(y * rows + p * step, step), step)
        residual = (
            stream_ref[piece, :].astype(f32) + (own_sum[own, :] + y_in[piece, :].astype(f32))
        ).astype(bf16)
        resid[piece, :] = residual
        tokens[sp, pl.ds(pl.multiple_of(tp * rows + p * step, step), step), :] = scaled_norm(
            residual.astype(f32), gain_ref[...].reshape(1, width)
        ).astype(bf16)
        pass_on(4, sp, y, p).start()
        along_z(sp, y, p)
        pass_on(2, sp, y, p).start()
        pass_on(3, sp, y, p).start()

    for load in loads[1:]:
        load.wait()

    def wait_piece(group, yy, p):
        pass_on(2, group, yy, p).wait_recv()

    def wait_mate(group, yy):
        block = block_of(group, yy, 1 - c)
        remote(block, block, tok_send.at[3, group, yy], mate_recv.at[group, yy], at(sp, sibling)).wait_recv()

    def block_at(code):
        relative, second, p = lax.div(code, 2 * PIECES), lax.rem(lax.div(code, PIECES), 2), lax.rem(code, PIECES)
        return relative, height_of(relative), jnp.where(second == 0, y, 1 - y), p

    def take(code):
        relative, height, yy, p = block_at(code)
        group = 2 * height + x
        wait_piece(group, yy, p)

        @pl.when((relative > 0) | at_end)
        def _():
            along_z(group, yy, p)

        pass_on(3, group, yy, p).start()

        @pl.when(relative > 0)
        def _():
            pass_on(2, group, yy, p).start()

    def take_across(code):
        _, height, yy, p = block_at(code)
        group = 2 * height + 1 - x
        wait_piece(group, yy, p)
        pass_on(3, group, yy, p).start()

    def pass_held(code):
        p = lax.rem(code, PIECES)

        @pl.when(code < PIECES)
        def _():
            pass_on(2, sp, 1 - y, p).start()

        @pl.when(code >= PIECES)
        def _():
            along_z(sp, 1 - y, p)

    def tile_at(tile):
        height = height_of(lax.div(tile, 4))
        side = jnp.where(lax.rem(lax.div(tile, 2), 2) == 0, x, 1 - x)
        return height, 2 * height + side, jnp.where(lax.rem(tile, 2) == 0, y, 1 - y)

    def tile_rows(yy):
        return pl.ds(pl.multiple_of(yy * half, half), half)

    def share(way, group, yy):
        whose = tp if way < 2 else opposite
        block = hidden.at[group, whose, tile_rows(yy), :]
        return remote(
            block,
            block,
            hid_send.at[way, group, yy],
            hid_recv.at[group, whose, yy],
            at(sp, sibling if way else opposite),
        )

    def wait_shared(group, whose, yy):
        block = hidden.at[group, whose, tile_rows(yy), :]
        remote(block, block, hid_send.at[0, group, yy], hid_recv.at[group, whose, yy], at(sp, sibling)).wait_recv()

    def gated_units(tile):
        _, group, yy = tile_at(tile)
        wait_mate(group, yy)
        inputs = tokens[group, tile_rows(yy), :]
        span = min(256, units)
        for start in range(0, units, span):
            gate_pre = jnp.dot(inputs, gate_w[:, start : start + span], preferred_element_type=f32)
            up_pre = jnp.dot(inputs, up_w[:, start : start + span], preferred_element_type=f32)
            hidden[group, tp, tile_rows(yy), start : start + span] = clamped_units(gate_pre, up_pre).astype(bf16)
        share(0, group, yy).start()
        share(1, group, yy).start()

    def relay_units(tile):
        _, group, yy = tile_at(tile)
        wait_shared(group, opposite, yy)
        share(2, group, yy).start()

    def chain_copy(group, yy):
        rising = lax.div(group, 2) > z
        return remote(
            part.at[group, tile_rows(yy), :],
            chain_in.at[jnp.where(rising, 0, 1), group, tile_rows(yy), :],
            chain_send.at[group, yy],
            chain_recv.at[jnp.where(rising, 0, 1), group, yy],
            at(sp + jnp.where(rising, 2, -2), tp),
        )

    def wait_chain(side, group, yy):
        block = chain_in.at[side, group, tile_rows(yy), :]
        remote(
            block, block, chain_send.at[group, yy], chain_recv.at[side, group, yy], at(sp, sibling)
        ).wait_recv()

    diagonal = lax.broadcasted_iota(jnp.int32, (half, half), 0) == lax.broadcasted_iota(jnp.int32, (half, half), 1)

    def project_down(tile):
        height, group, yy = tile_at(tile)
        wait_shared(group, sibling, yy)
        wait_shared(group, 3 - tp, yy)
        own_rows = tile_rows(yy)
        out = jnp.dot(hidden[group, 0, own_rows, :], down_w[:units, :], preferred_element_type=f32)
        for k in range(1, 4):
            out = out + jnp.dot(
                hidden[group, k, own_rows, :], down_w[k * units : (k + 1) * units, :], preferred_element_type=f32
            )
        weight = scales[group, :, tile_rows(yy)]
        mine = lax.broadcasted_iota(jnp.int32, weight.shape, 0) == sp
        weight = jnp.sum(jnp.where(mine, weight, 0.0), axis=0, keepdims=True)
        weight = jnp.sum(jnp.where(diagonal, weight, 0.0), axis=1, keepdims=True)
        part[group, own_rows, :] = (out.astype(bf16).astype(f32) * weight).astype(bf16)

        @pl.when(((height > z) & (z == 0)) | ((height < z) & (z == last)))
        def _():
            chain_copy(group, yy).start()

    def x_copy(group, yy):
        return remote(
            part.at[group, tile_rows(yy), :], x_in.at[tile_rows(yy), :], x_send.at[yy], x_recv.at[yy], at(across, tp)
        )

    def hand_over(to):
        return remote(
            final.at[pl.ds(to * rows, rows), :], columns.at[tp], fin_send.at[to], fin_recv.at[tp], at(sp, to)
        )

    def toward_home(tile):
        height, group, yy = tile_at(tile)
        own_rows = tile_rows(yy)
        total[...] = part[group, own_rows, :].astype(f32)
        for side, comes in enumerate(((height >= z) & (z > 0), (height <= z) & (z < last))):

            @pl.when(comes)
            def _():
                wait_chain(side, group, yy)
                total[...] = total[...] + chain_in[side, group, own_rows, :].astype(f32)

        @pl.when(group != sp)
        def _():
            part[group, own_rows, :] = total[...].astype(bf16)

            @pl.when(height != z)
            def _():
                chain_copy(group, yy).start()

            @pl.when(height == z)
            def _():
                x_copy(group, yy).start()

        @pl.when(group == sp)
        def _():
            x_copy(group, yy).wait_recv()
            final[own_rows, :] = (total[...] + x_in[own_rows, :].astype(f32)).astype(bf16)
            for to in range(4):

                @pl.when((tp != to) & (yy == to // 2))
                def _():
                    hand_over(to).start()

    acts = (take, take_across, pass_held, gated_units, relay_units, project_down, toward_home)

    def four_events(position, carry):
        word = pick(at_end, plans, position)

        def event(i, carry):
            code = lax.shift_right_logical(word, 8 * i) & 255
            kind, rest = lax.div(code, 32), lax.rem(code, 32)
            for j, act in enumerate(acts):

                @pl.when(kind == j)
                def _():
                    act(rest)

            return carry

        return lax.fori_loop(0, 4, event, carry)

    plans = [words_of(plan) for plan in (end_plan, middle_plan)]
    lax.fori_loop(0, max(len(plan) for plan in plans), four_events, 0)

    columns[tp] = final[pl.ds(pl.multiple_of(tp * rows, rows), rows), :]
    for by in (1, 2, 3):
        whose = lax.rem(tp + by, 4)
        remote(
            final.at[pl.ds(0, rows), :], columns.at[whose], fin_send.at[0], fin_recv.at[whose], at(sp, sibling)
        ).wait_recv()
    combined = jnp.concatenate([columns[k] for k in range(4)], 1).astype(f32)
    result_ref[...] = (
        resid[...].astype(f32) + scaled_norm(combined, post_gain_ref[...].reshape(1, width))
    ).astype(bf16)

    @pl.when(sp < sp_count - 1)
    def _():
        rim_copy.wait_send()

    remote(y_send, y_in, y_sem.at[0], y_recv.at[0], at(sp, opposite)).wait_send()
    sent(4, sp, y).wait_send()
    for to in range(4):

        @pl.when(tp != to)
        def _():
            hand_over(to).wait_send()

    def drain(group, carry):
        height = lax.div(group, 2)

        @pl.when(lax.rem(group, 2) == x)
        def _():
            for way in range(2):

                @pl.when(routes[way](group))
                def _():
                    scale_copy(way, group).wait_send()
                    for yy in range(2):
                        sent(way, group, yy).wait_send()

            scale_copy(2, group).wait_send()
            for yy in range(2):
                sent(2, group, yy).wait_send()

        for yy in range(2):
            sent(3, group, yy).wait_send()
            for way in range(3):
                share(way, group, yy).wait_send()

            @pl.when(height != z)
            def _():
                chain_copy(group, yy).wait_send()

            @pl.when((height == z) & (group != sp))
            def _():
                x_copy(group, yy).wait_send()

        return carry

    lax.fori_loop(0, sp_count, drain, 0)


def dense_layer(
    stream_in,
    pre_gate,
    value_in,
    post_gate,
    conv_taps,
    out_weight,
    route_ids,
    route_weight,
    ffn_gain,
    post_gain,
    gate_proj,
    up_proj,
    down_proj,
):
    sp_count = lax.axis_size("sp")
    rows, width = stream_in.shape
    seq, channels = pre_gate.shape
    units = gate_proj.shape[2]
    cols = down_proj.shape[2]
    bf16, f32 = jnp.bfloat16, jnp.float32
    dma = pltpu.SemaphoreType.DMA
    scratch = [
        pltpu.VMEM(out_weight.shape, bf16),
        pltpu.VMEM(gate_proj.shape[1:], bf16),
        pltpu.VMEM(up_proj.shape[1:], bf16),
        pltpu.VMEM(down_proj.shape[1:], bf16),
        pltpu.VMEM((16, channels), bf16),
        pltpu.VMEM((16, channels), bf16),
        pltpu.VMEM((seq + 8, channels), f32),
        pltpu.VMEM((seq, channels), bf16),
        pltpu.VMEM((2 * rows, width), bf16),
        pltpu.VMEM((2 * rows, width), bf16),
        pltpu.VMEM((2 * rows, width), f32),
        pltpu.VMEM((rows, width), bf16),
        pltpu.VMEM((rows, width), bf16),
        pltpu.VMEM((rows, width), bf16),
        pltpu.VMEM((sp_count, sp_count, seq), f32),
        pltpu.VMEM((sp_count, seq, width), bf16),
        pltpu.VMEM((sp_count, 4, seq, units), bf16),
        pltpu.VMEM((sp_count, seq, cols), bf16),
        pltpu.VMEM((2, sp_count, seq, cols), bf16),
        pltpu.VMEM((seq, cols), bf16),
        pltpu.VMEM((2 * rows, cols), f32),
        pltpu.VMEM((seq, cols), bf16),
        pltpu.VMEM((4, rows, cols), bf16),
        dma((4,)),
        dma((2,)),
        dma((2,)),
        dma((1,)),
        dma((PIECES,)),
        dma((3, sp_count)),
        dma((sp_count,)),
        dma((5, sp_count, 2)),
        dma((sp_count, 2, PIECES)),
        dma((sp_count, 2)),
        dma((3, sp_count, 2)),
        dma((sp_count, 4, 2)),
        dma((sp_count, 2)),
        dma((2, sp_count, 2)),
        dma((2,)),
        dma((2,)),
        dma((4,)),
        dma((4,)),
    ]
    vmem = pl.BlockSpec(memory_space=pltpu.VMEM)
    anywhere = pl.BlockSpec(memory_space=pl.ANY)
    return pl.pallas_call(
        functools.partial(layer_kernel, sp_count),
        out_shape=jax.ShapeDtypeStruct((rows, width), bf16),
        in_specs=[vmem] * 9 + [anywhere] * 4,
        out_specs=vmem,
        scratch_shapes=scratch,
        compiler_params=pltpu.CompilerParams(
            collective_id=0, has_side_effects=True, vmem_limit_bytes=58 * 1024 * 1024
        ),
    )(
        stream_in,
        pre_gate,
        value_in,
        post_gate,
        conv_taps,
        route_ids.T,
        route_weight.T,
        ffn_gain,
        post_gain,
        out_weight,
        gate_proj,
        up_proj,
        down_proj,
    )


def local(
    stream_in,
    pre_gate,
    value_in,
    post_gate,
    conv_taps,
    out_weight,
    route_ids,
    route_weight,
    ffn_gain,
    post_gain,
    gate_proj,
    up_proj,
    down_proj,
):
    sp_count = lax.axis_size("sp")
    tp_count = lax.axis_size("tp")
    seq_rows = pre_gate.shape[0]
    own_rows = seq_rows // tp_count
    top_count = route_ids.shape[1]
    slots_each = 2 * own_rows * top_count // sp_count
    if tp_count == 4 and sp_count == PLANNED_GROUPS and slots_each >= own_rows:
        return dense_layer(
            stream_in, pre_gate, value_in, post_gate, conv_taps, out_weight, route_ids, route_weight,
            ffn_gain, post_gain, gate_proj, up_proj, down_proj,
        )
    tap_count = conv_taps.shape[0]
    gated_input = (pre_gate.astype(jnp.float32) * value_in.astype(jnp.float32)).astype(jnp.bfloat16)
    rim_rows = passed_along(gated_input[seq_rows - tap_count + 1 :], "sp", 1)
    padded = jnp.concatenate([rim_rows, gated_input], 0).astype(jnp.float32)
    convolved = jnp.zeros(gated_input.shape, jnp.float32)
    for tap_index in range(tap_count):
        convolved = (
            convolved
            + conv_taps[tap_index].astype(jnp.float32)[None, :]
            * padded[tap_index : tap_index + seq_rows]
        )
    mixer_out = (post_gate.astype(jnp.float32) * convolved).astype(jnp.bfloat16)
    weight_rows = mixer_out
    projected = lax.psum_scatter(
        jnp.dot(weight_rows, out_weight, preferred_element_type=jnp.float32),
        "tp",
        scatter_dimension=0,
        tiled=True,
    )
    residual = (stream_in.astype(jnp.float32) + projected).astype(jnp.bfloat16)
    normed = scaled_norm(residual.astype(jnp.float32), ffn_gain).astype(jnp.bfloat16)
    slot_rank = block_ranks(route_ids, sp_count, own_rows)
    block_of = (jnp.arange(seq_rows, dtype=jnp.int32) // own_rows)[:, None]
    tp_index = lax.axis_index("tp")
    own_ids = lax.dynamic_slice_in_dim(route_ids, tp_index * own_rows, own_rows, 0)
    own_rank = lax.dynamic_slice_in_dim(slot_rank, tp_index * own_rows, own_rows, 0)
    own_slot = own_ids * slots_each + own_rank
    picker = slot_picker(own_slot, sp_count * slots_each)
    outgoing = jnp.dot(picker, normed, preferred_element_type=jnp.float32).astype(jnp.bfloat16)
    arrived = lax.all_to_all(outgoing, "sp", split_axis=0, concat_axis=0, tiled=True)
    portion = lax.all_gather(arrived, "tp", axis=0, tiled=True)
    gate_pre = jnp.dot(portion, gate_proj[0], preferred_element_type=jnp.float32)
    up_pre = jnp.dot(portion, up_proj[0], preferred_element_type=jnp.float32)
    hidden = clamped_units(gate_pre, up_pre).astype(jnp.bfloat16)
    weight_rows = down_proj[0]
    column_out = jnp.dot(
        lax.all_gather(hidden, "tp", axis=1, tiled=True),
        weight_rows,
        preferred_element_type=jnp.float32,
    ).astype(jnp.bfloat16)
    column_width = column_out.shape[1]
    returned = lax.all_to_all(
        column_out.reshape(tp_count, sp_count, slots_each, column_width),
        "sp",
        split_axis=1,
        concat_axis=1,
        tiled=True,
    )
    home_index = (block_of * sp_count + route_ids) * slots_each + slot_rank
    gathered_out = jnp.take(returned.reshape(-1, column_width), home_index.reshape(-1), axis=0)
    gathered_out = gathered_out.astype(jnp.float32).reshape(seq_rows, top_count, column_width)
    combined_cols = jnp.sum(gathered_out * route_weight[:, :, None], axis=1).astype(jnp.bfloat16)
    combined = lax.all_to_all(combined_cols, "tp", split_axis=0, concat_axis=1, tiled=True)
    layer_out = residual.astype(jnp.float32) + scaled_norm(combined.astype(jnp.float32), post_gain)
    return layer_out.astype(jnp.bfloat16)


def solution(mesh):
    placed = (
        P(("sp", "tp"), None),
        P("sp", "tp"),
        P("sp", "tp"),
        P("sp", "tp"),
        P(None, "tp"),
        P("tp", None),
        P("sp", None),
        P("sp", None),
        P(),
        P(),
        P("sp", None, "tp"),
        P("sp", None, "tp"),
        P("sp", None, "tp"),
    )
    return jax.shard_map(
        local, mesh=mesh, in_specs=placed, out_specs=P(("sp", "tp"), None), check_vma=False
    )
```

time: 111 us -> 93.6 us (0.84)
  the two profiles are of different devices: /device:TPU:1 before, /device:TPU:9 now
where the time goes in v1:
time: 93.6 us; the launch traced here: 93.4 us
  Pallas kernels  91.8 us (98%)
  local copies, waits for them, and re-layouts  1.67 us (2%)
    pallas_call x1, Pallas kernels, dense_layer(): pl.pallas_call(functools.partial(layer_kernel, sp_count), out_shape=jax.S...  91.8 us

profile of v1, /device:TPU:9, one launch (start us, length us, event | category | flops | bytes accessed | tf_op | source)
XLA Modules:
  0.0 93.4 jit_solution(8164813647160346841)
XLA Ops:
  0.0 91.8 %shard_map.127 = bf16[64,2048]{1,0:T(8,128)(2,1)} custom-call(bf16[64,2048]{1,0:T(8,128)(2,1)} %stream_ref.1, bf16[256,256]{1,0:T(8,128)(2,1)} %pre_ref.1, bf16[256,256]{1,0:T(8,128)(2,1)} %value_ref.1, bf16[256,256]{1,0:T(8,128)(2,1)} %post_ref.1, bf16[3,256]{1,0:T(4,128)(2,1)} %taps_ref.1, s32[4,256]{1,0:T(4,128)} %bitcast.2, f32[4,256]{1,0:T(4,128)} %bitcast.3, ...), custom_call_target="tpu_custom_call" | custom-call | tf_op jit(solution)/shard_map/pallas_call | solution.py:648
  91.8 1.7 %copy.15 = bf16[64,2048]{1,0:T(8,128)(2,1)} copy(bf16[64,2048]{1,0:T(8,128)(2,1)} %shard_map.127) | data formatting | bytes 524288

commit v2 on v1

--- a/solution.py
+++ b/solution.py
@@ -135,6 +135,7 @@
     mate_recv,
     hid_send,
     hid_recv,
+    mate_hid_recv,
     chain_send,
     chain_recv,
     x_send,
@@ -219,7 +220,7 @@
     devices = (at(sp + 2, tp), at(sp - 2, tp), at(across, tp), at(sp, sibling), at(sp, opposite))
 
     def scale_copy(way, group):
-        return remote(scales.at[group], scales.at[group], scale_send.at[way, group], scale_recv.at[group], devices[way])
+        return remote(scales.at[group], scales.at[group], scale_send.at[way], scale_recv.at[group], devices[way])
 
     def send_scales(group):
         for way in range(2):
@@ -280,20 +281,6 @@
     def wait_scales(group):
         scale_copy(2, group).wait_recv()
 
-    def take_scales(relative, carry):
-        group = 2 * height_of(relative) + x
-        wait_scales(group)
-        send_scales(group)
-        return carry
-
-    lax.fori_loop(1, heights, take_scales, 0)
-
-    def take_scales_across(height, carry):
-        wait_scales(2 * height + 1 - x)
-        return carry
-
-    lax.fori_loop(0, heights, take_scales_across, 0)
-
     def piece_of(group, yy, p):
         return tokens.at[group, pl.ds(pl.multiple_of((2 * yy + c) * rows + p * step, step), step), :]
 
@@ -303,11 +290,11 @@
     def pass_on(way, group, yy, p):
         piece = piece_of(group, yy, p)
         receive = mate_recv.at[group, yy] if way == 3 else tok_recv.at[group, yy, p]
-        return remote(piece, piece, tok_send.at[way, group, yy], receive, devices[way])
-
-    def sent(way, group, yy):
-        block = block_of(group, yy, c)
-        return remote(block, block, tok_send.at[way, group, yy], mate_recv.at[group, yy], devices[way])
+        return remote(piece, piece, tok_send.at[way], receive, devices[way])
+
+    def sent(way, group_count, row_count):
+        rows_sent = tokens.at[pl.ds(0, group_count), pl.ds(0, row_count), :]
+        return remote(rows_sent, rows_sent, tok_send.at[way], mate_recv.at[0, 0], devices[way])
 
     def along_z(group, yy, p):
         for way in range(2):
@@ -340,7 +327,7 @@
 
     def wait_mate(group, yy):
         block = block_of(group, yy, 1 - c)
-        remote(block, block, tok_send.at[3, group, yy], mate_recv.at[group, yy], at(sp, sibling)).wait_recv()
+        remote(block, block, tok_send.at[3], mate_recv.at[group, yy], at(sp, sibling)).wait_recv()
 
     def block_at(code):
         relative, second, p = lax.div(code, 2 * PIECES), lax.rem(lax.div(code, PIECES), 2), lax.rem(code, PIECES)
@@ -349,6 +336,12 @@
     def take(code):
         relative, height, yy, p = block_at(code)
         group = 2 * height + x
+
+        @pl.when((relative > 0) & (lax.rem(code, 2 * PIECES) == 0))
+        def _():
+            wait_scales(group)
+            send_scales(group)
+
         wait_piece(group, yy, p)
 
         @pl.when((relative > 0) | at_end)
@@ -364,6 +357,11 @@
     def take_across(code):
         _, height, yy, p = block_at(code)
         group = 2 * height + 1 - x
+
+        @pl.when(lax.rem(code, 2 * PIECES) == 0)
+        def _():
+            wait_scales(group)
+
         wait_piece(group, yy, p)
         pass_on(3, group, yy, p).start()
 
@@ -389,17 +387,8 @@
     def share(way, group, yy):
         whose = tp if way < 2 else opposite
         block = hidden.at[group, whose, tile_rows(yy), :]
-        return remote(
-            block,
-            block,
-            hid_send.at[way, group, yy],
-            hid_recv.at[group, whose, yy],
-            at(sp, sibling if way else opposite),
-        )
-
-    def wait_shared(group, whose, yy):
-        block = hidden.at[group, whose, tile_rows(yy), :]
-        remote(block, block, hid_send.at[0, group, yy], hid_recv.at[group, whose, yy], at(sp, sibling)).wait_recv()
+        receive = mate_hid_recv.at[group, yy] if way else hid_recv.at[group, yy]
+        return remote(block, block, hid_send.at[way], receive, at(sp, sibling if way else opposite))
 
     def gated_units(tile):
         _, group, yy = tile_at(tile)
@@ -415,7 +404,7 @@
 
     def relay_units(tile):
         _, group, yy = tile_at(tile)
-        wait_shared(group, opposite, yy)
+        share(0, group, yy).wait_recv()
         share(2, group, yy).start()
 
     def chain_copy(group, yy):
@@ -423,23 +412,21 @@
         return remote(
             part.at[group, tile_rows(yy), :],
             chain_in.at[jnp.where(rising, 0, 1), group, tile_rows(yy), :],
-            chain_send.at[group, yy],
-            chain_recv.at[jnp.where(rising, 0, 1), group, yy],
+            chain_send.at[0],
+            chain_recv.at[group, yy],
             at(sp + jnp.where(rising, 2, -2), tp),
         )
 
-    def wait_chain(side, group, yy):
-        block = chain_in.at[side, group, tile_rows(yy), :]
-        remote(
-            block, block, chain_send.at[group, yy], chain_recv.at[side, group, yy], at(sp, sibling)
-        ).wait_recv()
+    def wait_chain(sides, group, yy):
+        tiles = chain_in.at[pl.ds(0, sides), group, tile_rows(yy), :]
+        remote(tiles, tiles, chain_send.at[0], chain_recv.at[group, yy], at(sp, sibling)).wait_recv()
 
     diagonal = lax.broadcasted_iota(jnp.int32, (half, half), 0) == lax.broadcasted_iota(jnp.int32, (half, half), 1)
 
     def project_down(tile):
         height, group, yy = tile_at(tile)
-        wait_shared(group, sibling, yy)
-        wait_shared(group, 3 - tp, yy)
+        both = hidden.at[group, pl.ds(0, 2), tile_rows(yy), :]
+        remote(both, both, hid_send.at[1], mate_hid_recv.at[group, yy], at(sp, sibling)).wait_recv()
         own_rows = tile_rows(yy)
         out = jnp.dot(hidden[group, 0, own_rows, :], down_w[:units, :], preferred_element_type=f32)
         for k in range(1, 4):
@@ -458,23 +445,32 @@
 
     def x_copy(group, yy):
         return remote(
-            part.at[group, tile_rows(yy), :], x_in.at[tile_rows(yy), :], x_send.at[yy], x_recv.at[yy], at(across, tp)
+            part.at[group, tile_rows(yy), :], x_in.at[tile_rows(yy), :], x_send.at[0], x_recv.at[yy], at(across, tp)
         )
 
     def hand_over(to):
         return remote(
-            final.at[pl.ds(to * rows, rows), :], columns.at[tp], fin_send.at[to], fin_recv.at[tp], at(sp, to)
+            final.at[pl.ds(to * rows, rows), :], columns.at[tp], fin_send.at[0], fin_recv.at[tp], at(sp, to)
         )
 
     def toward_home(tile):
         height, group, yy = tile_at(tile)
         own_rows = tile_rows(yy)
         total[...] = part[group, own_rows, :].astype(f32)
+        both_sides = (height == z) & jnp.logical_not(at_end)
+
+        @pl.when(both_sides)
+        def _():
+            wait_chain(2, group, yy)
+
+        @pl.when(jnp.logical_not(both_sides))
+        def _():
+            wait_chain(1, group, yy)
+
         for side, comes in enumerate(((height >= z) & (z > 0), (height <= z) & (z < last))):
 
             @pl.when(comes)
             def _():
-                wait_chain(side, group, yy)
                 total[...] = total[...] + chain_in[side, group, own_rows, :].astype(f32)
 
         @pl.when(group != sp)
@@ -536,46 +532,32 @@
         rim_copy.wait_send()
 
     remote(y_send, y_in, y_sem.at[0], y_recv.at[0], at(sp, opposite)).wait_send()
-    sent(4, sp, y).wait_send()
-    for to in range(4):
-
-        @pl.when(tp != to)
-        def _():
-            hand_over(to).wait_send()
-
-    def drain(group, carry):
-        height = lax.div(group, 2)
-
-        @pl.when(lax.rem(group, 2) == x)
-        def _():
-            for way in range(2):
-
-                @pl.when(routes[way](group))
-                def _():
-                    scale_copy(way, group).wait_send()
-                    for yy in range(2):
-                        sent(way, group, yy).wait_send()
-
-            scale_copy(2, group).wait_send()
-            for yy in range(2):
-                sent(2, group, yy).wait_send()
-
-        for yy in range(2):
-            sent(3, group, yy).wait_send()
-            for way in range(3):
-                share(way, group, yy).wait_send()
-
-            @pl.when(height != z)
+    sent(4, 1, rows).wait_send()
+    sent(3, heights, seq).wait_send()
+    sent(2, heights, half).wait_send()
+
+    def scales_sent(way, group_count):
+        blocks = scales.at[pl.ds(0, group_count)]
+        remote(blocks, blocks, scale_send.at[way], scale_recv.at[0], devices[way]).wait_send()
+
+    scales_sent(2, heights)
+    for count in range(1, heights):
+        for way, its in enumerate((z == count - 1, z == heights - count)):
+
+            @pl.when(its)
             def _():
-                chain_copy(group, yy).wait_send()
-
-            @pl.when((height == z) & (group != sp))
-            def _():
-                x_copy(group, yy).wait_send()
-
-        return carry
-
-    lax.fori_loop(0, sp_count, drain, 0)
+                sent(way, count, half).wait_send()
+                scales_sent(way, count)
+
+    for way in range(3):
+        tiles = hidden.at[:, 0]
+        receive = mate_hid_recv.at[0, 0] if way else hid_recv.at[0, 0]
+        remote(tiles, tiles, hid_send.at[way], receive, at(sp, sibling)).wait_send()
+    chained = part.at[pl.ds(0, sp_count - 2)]
+    remote(chained, chained, chain_send.at[0], chain_recv.at[0, 0], at(sp, sibling)).wait_send()
+    remote(part.at[0], x_in, x_send.at[0], x_recv.at[0], at(across, tp)).wait_send()
+    handed = final.at[pl.ds(0, 3 * rows), :]
+    remote(handed, handed, fin_send.at[0], fin_recv.at[0], at(sp, sibling)).wait_send()
 
 
 def dense_layer(
@@ -629,18 +611,19 @@
         dma((2,)),
         dma((1,)),
         dma((PIECES,)),
-        dma((3, sp_count)),
+        dma((3,)),
         dma((sp_count,)),
-        dma((5, sp_count, 2)),
+        dma((5,)),
         dma((sp_count, 2, PIECES)),
         dma((sp_count, 2)),
-        dma((3, sp_count, 2)),
-        dma((sp_count, 4, 2)),
+        dma((3,)),
         dma((sp_count, 2)),
-        dma((2, sp_count, 2)),
+        dma((sp_count, 2)),
+        dma((1,)),
+        dma((sp_count, 2)),
+        dma((1,)),
         dma((2,)),
-        dma((2,)),
-        dma((4,)),
+        dma((1,)),
         dma((4,)),
     ]
     vmem = pl.BlockSpec(memory_space=pltpu.VMEM)

time: 93.6 us -> 88.5 us (0.946)
  Pallas kernels: 91.8 us -> 86.7 us
    pallas_call x1, Pallas kernels: 91.8 us -> 86.7 us  [dense_layer(): pl.pallas_call(functools.partial(layer_kernel, sp_count), out_shape=jax.S...]
where the time goes in v2:
time: 88.5 us; the launch traced here: 88.3 us
  Pallas kernels  86.7 us (98%)
  local copies, waits for them, and re-layouts  1.67 us (2%)
    pallas_call x1, Pallas kernels, dense_layer(): pl.pallas_call(functools.partial(layer_kernel, sp_count), out_shape=jax.S...  86.7 us

profile of v2, /device:TPU:9, one launch (start us, length us, event | category | flops | bytes accessed | tf_op | source)
XLA Modules:
  0.0 88.3 jit_solution(17117844032718760656)
XLA Ops:
  0.0 86.7 %shard_map.127 = bf16[64,2048]{1,0:T(8,128)(2,1)} custom-call(bf16[64,2048]{1,0:T(8,128)(2,1)} %stream_ref.1, bf16[256,256]{1,0:T(8,128)(2,1)} %pre_ref.1, bf16[256,256]{1,0:T(8,128)(2,1)} %value_ref.1, bf16[256,256]{1,0:T(8,128)(2,1)} %post_ref.1, bf16[3,256]{1,0:T(4,128)(2,1)} %taps_ref.1, s32[4,256]{1,0:T(4,128)} %bitcast.2, f32[4,256]{1,0:T(4,128)} %bitcast.3, ...), custom_call_target="tpu_custom_call" | custom-call | tf_op jit(solution)/shard_map/pallas_call | solution.py:631
  86.7 1.7 %copy.15 = bf16[64,2048]{1,0:T(8,128)(2,1)} copy(bf16[64,2048]{1,0:T(8,128)(2,1)} %shard_map.127) | data formatting | bytes 524288

commit v3 on v2

--- a/solution.py
+++ b/solution.py
@@ -50,21 +50,21 @@
 PIECES = 4
 PLANNED_GROUPS = 8
 end_plan = (
-    32, 33, 4, 8, 10, 5, 96, 11, 35, 6, 16, 7, 34, 18, 98, 19, 43, 9, 17, 97,
-    104, 26, 24, 48, 25, 27, 51, 49, 42, 41, 40, 50, 131, 108, 31, 28, 106, 30, 29, 66,
-    58, 57, 64, 109, 56, 59, 137, 141, 110, 173, 60, 63, 62, 67, 61, 65, 140, 111, 172, 22,
-    38, 23, 102, 143, 129, 39, 21, 20, 36, 15, 175, 142, 105, 55, 37, 174, 13, 12, 99, 53,
-    54, 52, 139, 135, 14, 169, 107, 128, 136, 101, 171, 161, 130, 44, 168, 47, 45, 163, 46, 138,
-    103, 170, 100, 160, 167, 162, 134, 132, 166, 194, 133, 164, 165, 195, 192, 193,
+    8, 9, 11, 10, 34, 5, 6, 40, 96, 16, 4, 7, 43, 18, 97, 32, 33, 35, 19, 42,
+    41, 98, 17, 26, 104, 27, 102, 25, 58, 24, 29, 59, 31, 129, 128, 30, 108, 28, 65, 64,
+    66, 56, 67, 137, 48, 51, 50, 61, 57, 49, 109, 110, 106, 62, 141, 63, 173, 22, 140, 161,
+    60, 172, 21, 111, 23, 143, 20, 175, 105, 13, 14, 131, 15, 54, 169, 39, 37, 53, 139, 142,
+    12, 36, 38, 135, 55, 52, 174, 107, 99, 45, 136, 171, 47, 168, 46, 44, 163, 138, 103, 170,
+    100, 160, 130, 101, 195, 162, 167, 134, 166, 133, 194, 165, 193, 132, 164, 192,
 )
 middle_plan = (
-    9, 8, 16, 18, 96, 19, 10, 17, 4, 34, 104, 24, 11, 26, 5, 6, 7, 12, 14, 15,
-    13, 25, 27, 100, 28, 108, 101, 31, 49, 51, 50, 48, 30, 29, 71, 109, 106, 68, 69, 97,
-    33, 70, 58, 47, 46, 141, 140, 44, 45, 23, 32, 22, 20, 21, 103, 137, 133, 59, 56, 105,
-    172, 57, 35, 165, 173, 60, 62, 63, 61, 40, 41, 111, 110, 136, 139, 42, 55, 43, 204, 129,
-    205, 132, 52, 54, 169, 65, 66, 64, 67, 142, 53, 102, 168, 174, 128, 134, 107, 143, 206, 166,
-    38, 197, 175, 135, 207, 171, 98, 167, 198, 37, 39, 36, 160, 138, 203, 161, 99, 199, 164, 170,
-    196, 202, 131, 163, 195, 130, 201, 162, 200, 194, 192, 193,
+    16, 8, 17, 10, 96, 18, 19, 11, 9, 104, 26, 33, 24, 27, 100, 25, 5, 13, 42, 6,
+    14, 15, 12, 4, 7, 108, 29, 30, 97, 31, 101, 28, 35, 32, 34, 70, 109, 59, 129, 56,
+    58, 69, 57, 41, 71, 141, 133, 43, 110, 68, 22, 21, 50, 51, 23, 48, 49, 132, 140, 20,
+    40, 102, 106, 44, 45, 60, 63, 61, 62, 46, 47, 173, 65, 66, 67, 143, 111, 172, 103, 55,
+    54, 139, 175, 207, 52, 205, 53, 64, 164, 135, 165, 107, 142, 128, 167, 105, 171, 137, 38, 199,
+    174, 206, 204, 36, 134, 37, 39, 138, 197, 98, 203, 99, 166, 198, 136, 170, 161, 202, 196, 131,
+    169, 168, 160, 201, 130, 163, 195, 162, 194, 200, 193, 192,
 )
 
 def words_of(plan):
@@ -126,6 +126,7 @@
     load_sem,
     rim_sem,
     pair_sem,
+    pair_recv,
     y_sem,
     y_recv,
     scale_send,
@@ -233,46 +234,84 @@
 
     send_scales(sp)
     padded[8:, :] = gated.astype(f32)
-
-    @pl.when(sp == 0)
+    padded[:8, :] = jnp.zeros((8, padded.shape[1]), f32)
+    tap_count = taps_ref.shape[0]
+    taps = taps_ref[...].astype(f32)
+
+    def mix(count):
+        convolved = jnp.zeros((count, padded.shape[1]), f32)
+        for k in range(tap_count):
+            first = 8 - tap_count + 1 + k
+            convolved = convolved + taps[k : k + 1, :] * padded[first : first + count, :]
+        mixed[:count, :] = (post_ref[:count, :].astype(f32) * convolved).astype(bf16)
+
+    mix(seq)
+    loads[0].wait()
+
+    def rows_of(core):
+        return jnp.concatenate(
+            [mixed[pl.ds(pl.multiple_of(yy * half + core * rows, rows), rows), :] for yy in range(2)], 0
+        )
+
+    def offset_of(p):
+        return lax.rem(p + 1, PIECES) * step
+
+    def pair_copy(i):
+        if i < 2:
+            whose = pl.ds(pl.multiple_of(((1 - y) if i == 0 else y) * rows + step, step), rows - step)
+        else:
+            whose = pl.ds((3 - i) * rows, step)
+        return remote(
+            pair_send.at[whose, :], pair_in.at[whose, :], pair_sem.at[0], pair_recv.at[i], at(sp, sibling)
+        )
+
+    pair_send[...] = jnp.dot(rows_of(1 - c), out_w[...], preferred_element_type=f32).astype(bf16)
+    for i in range(3):
+        pair_copy(i).start()
+
+    @pl.when(c == 0)
     def _():
-        padded[:8, :] = jnp.zeros((8, padded.shape[1]), f32)
+        pair_copy(3).start()
+
+    own_sum[...] = jnp.dot(rows_of(c), out_w[...], preferred_element_type=f32)
+
+    def pair_sum(yy, p):
+        piece = pl.ds(pl.multiple_of(yy * rows + offset_of(p), step), step)
+        return own_sum[piece, :] + pair_in[piece, :].astype(f32)
+
+    def y_copy(p):
+        piece = pl.ds(pl.multiple_of(offset_of(p), step), step)
+        return remote(y_send.at[piece, :], y_in.at[piece, :], y_sem.at[0], y_recv.at[p], at(sp, opposite))
+
+    def send_y(p):
+        y_send[pl.ds(pl.multiple_of(offset_of(p), step), step), :] = pair_sum(1 - y, p).astype(bf16)
+        y_copy(p).start()
+
+    pair_copy(0).wait_recv()
+    for p in range(PIECES - 1):
+        send_y(p)
 
     @pl.when(sp > 0)
     def _():
         rim_copy.wait_recv()
         padded[:8, :] = rim[...].astype(f32)[8:]
 
-    tap_count = taps_ref.shape[0]
-    taps = taps_ref[...].astype(f32)
-    convolved = jnp.zeros((seq, padded.shape[1]), f32)
-    for k in range(tap_count):
-        first = 8 - tap_count + 1 + k
-        convolved = convolved + taps[k : k + 1, :] * padded[first : first + seq, :]
-    mixed[...] = (post_ref[...].astype(f32) * convolved).astype(bf16)
-    loads[0].wait()
-
-    def rows_of(core):
-        return jnp.concatenate(
-            [mixed[pl.ds(pl.multiple_of(yy * half + core * rows, rows), rows), :] for yy in range(2)], 0
-        )
-
-    pair_send[...] = jnp.dot(rows_of(1 - c), out_w[...], preferred_element_type=f32).astype(bf16)
-    pair_copy = remote(pair_send, pair_in, pair_sem.at[0], pair_sem.at[1], at(sp, sibling))
-    pair_copy.start()
-    own_sum[...] = jnp.dot(rows_of(c), out_w[...], preferred_element_type=f32)
-    pair_copy.wait()
-    far = pl.ds(pl.multiple_of((1 - y) * rows, rows), rows)
-    near = pl.ds(pl.multiple_of(y * rows, rows), rows)
-    y_send[...] = (own_sum[far, :] + pair_in[far, :].astype(f32)).astype(bf16)
-
-    def y_copy(p):
-        piece = pl.ds(p * step, step)
-        return remote(y_send.at[piece, :], y_in.at[piece, :], y_sem.at[0], y_recv.at[p], at(sp, opposite))
-
-    for p in range(PIECES):
-        y_copy(p).start()
-    own_sum[near, :] = own_sum[near, :] + pair_in[near, :].astype(f32)
+    mix(step)
+    first_rows = jnp.dot(mixed[:step, :], out_w[...], preferred_element_type=f32)
+
+    @pl.when(c == 0)
+    def _():
+        own_sum[:step, :] = first_rows
+
+    @pl.when(c == 1)
+    def _():
+        pair_send[:step, :] = first_rows.astype(bf16)
+        pair_copy(3).start()
+
+    for i in (2, 3):
+        pair_copy(i).wait_recv()
+    send_y(PIECES - 1)
+    pair_copy(1).wait_recv()
 
     def height_of(relative):
         inner = jnp.where(relative == 0, 0, jnp.where(relative == 1, -1, relative - 1))
@@ -282,7 +321,7 @@
         scale_copy(2, group).wait_recv()
 
     def piece_of(group, yy, p):
-        return tokens.at[group, pl.ds(pl.multiple_of((2 * yy + c) * rows + p * step, step), step), :]
+        return tokens.at[group, pl.ds(pl.multiple_of((2 * yy + c) * rows + offset_of(p), step), step), :]
 
     def block_of(group, yy, core):
         return tokens.at[group, pl.ds(pl.multiple_of((2 * yy + core) * rows, rows), rows), :]
@@ -305,13 +344,12 @@
 
     for p in range(PIECES):
         y_copy(p).wait_recv()
-        piece = pl.ds(p * step, step)
-        own = pl.ds(pl.multiple_of(y * rows + p * step, step), step)
+        piece = pl.ds(pl.multiple_of(offset_of(p), step), step)
         residual = (
-            stream_ref[piece, :].astype(f32) + (own_sum[own, :] + y_in[piece, :].astype(f32))
+            stream_ref[piece, :].astype(f32) + (pair_sum(y, p) + y_in[piece, :].astype(f32))
         ).astype(bf16)
         resid[piece, :] = residual
-        tokens[sp, pl.ds(pl.multiple_of(tp * rows + p * step, step), step), :] = scaled_norm(
+        tokens[sp, pl.ds(pl.multiple_of(tp * rows + offset_of(p), step), step), :] = scaled_norm(
             residual.astype(f32), gain_ref[...].reshape(1, width)
         ).astype(bf16)
         pass_on(4, sp, y, p).start()
@@ -531,6 +569,7 @@
     def _():
         rim_copy.wait_send()
 
+    remote(pair_send, pair_in, pair_sem.at[0], pair_recv.at[0], at(sp, sibling)).wait_send()
     remote(y_send, y_in, y_sem.at[0], y_recv.at[0], at(sp, opposite)).wait_send()
     sent(4, 1, rows).wait_send()
     sent(3, heights, seq).wait_send()
@@ -608,7 +647,8 @@
         pltpu.VMEM((4, rows, cols), bf16),
         dma((4,)),
         dma((2,)),
-        dma((2,)),
+        dma((1,)),
+        dma((4,)),
         dma((1,)),
         dma((PIECES,)),
         dma((3,)),

time: 88.5 us -> 82.8 us (0.936)
  Pallas kernels: 86.7 us -> 80.6 us
    pallas_call x1, Pallas kernels: 86.7 us -> 80.6 us  [dense_layer(): pl.pallas_call(functools.partial(layer_kernel, sp_count), out_shape=jax.S...]
where the time goes in v3:
time: 82.8 us; the launch traced here: 82.3 us
  Pallas kernels  80.6 us (97%)
  local copies, waits for them, and re-layouts  1.67 us (2%)
    pallas_call x1, Pallas kernels, dense_layer(): pl.pallas_call(functools.partial(layer_kernel, sp_count), out_shape=jax.S...  80.6 us
    unnamed x1, local copies, waits for them, and re-layouts  1.67 us

profile of v3, /device:TPU:9, one launch (start us, length us, event | category | flops | bytes accessed | tf_op | source)
XLA Modules:
  0.0 82.3 jit_solution(7153711910076997713)
XLA Ops:
  0.0 80.6 %shard_map.127 = bf16[64,2048]{1,0:T(8,128)(2,1)} custom-call(bf16[64,2048]{1,0:T(8,128)(2,1)} %stream_ref.1, bf16[256,256]{1,0:T(8,128)(2,1)} %pre_ref.1, bf16[256,256]{1,0:T(8,128)(2,1)} %value_ref.1, bf16[256,256]{1,0:T(8,128)(2,1)} %post_ref.1, bf16[3,256]{1,0:T(4,128)(2,1)} %taps_ref.1, s32[4,256]{1,0:T(4,128)} %bitcast.2, f32[4,256]{1,0:T(4,128)} %bitcast.3, ...), custom_call_target="tpu_custom_call" | custom-call | tf_op jit(solution)/shard_map/pallas_call | solution.py:671
  80.6 1.7 %copy.15 = bf16[64,2048]{1,0:T(8,128)(2,1)} copy(bf16[64,2048]{1,0:T(8,128)(2,1)} %shard_map.127) | data formatting | bytes 524288

commit v4 on v3

--- a/solution.py
+++ b/solution.py
@@ -50,22 +50,42 @@
 PIECES = 4
 PLANNED_GROUPS = 8
 end_plan = (
-    8, 9, 11, 10, 34, 5, 6, 40, 96, 16, 4, 7, 43, 18, 97, 32, 33, 35, 19, 42,
-    41, 98, 17, 26, 104, 27, 102, 25, 58, 24, 29, 59, 31, 129, 128, 30, 108, 28, 65, 64,
-    66, 56, 67, 137, 48, 51, 50, 61, 57, 49, 109, 110, 106, 62, 141, 63, 173, 22, 140, 161,
-    60, 172, 21, 111, 23, 143, 20, 175, 105, 13, 14, 131, 15, 54, 169, 39, 37, 53, 139, 142,
-    12, 36, 38, 135, 55, 52, 174, 107, 99, 45, 136, 171, 47, 168, 46, 44, 163, 138, 103, 170,
-    100, 160, 130, 101, 195, 162, 167, 134, 166, 133, 194, 165, 193, 132, 164, 192,
+    8, 96, 10, 5, 11, 9, 4, 7, 100, 16, 6, 18, 19, 97, 42, 41, 17, 40, 43, 102,
+    24, 104, 27, 25, 26, 59, 50, 108, 31, 56, 29, 57, 30, 28, 58, 109, 48, 51, 49, 12,
+    141, 106, 14, 173, 218, 110, 63, 60, 133, 62, 135, 13, 219, 140, 15, 61, 20, 22, 111, 101,
+    172, 216, 165, 139, 129, 23, 21, 45, 217, 44, 143, 66, 65, 175, 105, 52, 47, 54, 35, 137,
+    223, 33, 46, 67, 142, 64, 55, 128, 53, 32, 222, 174, 221, 107, 103, 161, 34, 171, 215, 167,
+    214, 98, 207, 132, 39, 206, 169, 220, 138, 36, 136, 38, 37, 211, 210, 170, 213, 99, 203, 134,
+    212, 168, 166, 204, 202, 205, 209, 131, 163, 199, 164, 198, 130, 208, 200, 201, 162, 197, 160, 195,
+    196, 194, 193, 192,
 )
 middle_plan = (
-    16, 8, 17, 10, 96, 18, 19, 11, 9, 104, 26, 33, 24, 27, 100, 25, 5, 13, 42, 6,
-    14, 15, 12, 4, 7, 108, 29, 30, 97, 31, 101, 28, 35, 32, 34, 70, 109, 59, 129, 56,
-    58, 69, 57, 41, 71, 141, 133, 43, 110, 68, 22, 21, 50, 51, 23, 48, 49, 132, 140, 20,
-    40, 102, 106, 44, 45, 60, 63, 61, 62, 46, 47, 173, 65, 66, 67, 143, 111, 172, 103, 55,
-    54, 139, 175, 207, 52, 205, 53, 64, 164, 135, 165, 107, 142, 128, 167, 105, 171, 137, 38, 199,
-    174, 206, 204, 36, 134, 37, 39, 138, 197, 98, 203, 99, 166, 198, 136, 170, 161, 202, 196, 131,
-    169, 168, 160, 201, 130, 163, 195, 162, 194, 200, 193, 192,
+    16, 8, 4, 17, 96, 10, 11, 18, 6, 9, 19, 13, 100, 24, 27, 5, 7, 97, 25, 15,
+    26, 14, 29, 12, 35, 34, 108, 42, 40, 31, 41, 30, 101, 28, 68, 133, 128, 70, 129, 69,
+    43, 109, 32, 104, 71, 102, 132, 59, 22, 33, 57, 161, 98, 160, 20, 58, 141, 21, 51, 56,
+    48, 23, 140, 49, 65, 50, 173, 110, 172, 62, 61, 64, 105, 66, 67, 218, 47, 131, 63, 46,
+    44, 60, 143, 45, 111, 219, 106, 103, 175, 54, 55, 53, 52, 165, 217, 135, 216, 164, 142, 223,
+    107, 222, 174, 139, 167, 202, 137, 36, 38, 221, 37, 39, 207, 171, 215, 136, 134, 99, 206, 203,
+    214, 166, 163, 220, 199, 138, 198, 205, 168, 170, 200, 169, 211, 213, 212, 210, 204, 130, 162, 201,
+    197, 196, 209, 194, 208, 195, 193, 192,
 )
+x_first = (
+    ((1, 0), (1, 1), (2, 0),),
+    ((2, 0), (2, 1),),
+)
+
+def comes_along_z(x_first_end, x_first_middle):
+    near, far = [0, 0], [0, 0]
+    for tile in range(16):
+        height, across, second = tile // 4, tile // 2 % 2, tile % 2
+        if height == 0 and not (across and (1, second) in x_first_middle):
+            far[0] |= 1 << tile
+        if not (across and (height or 1, second) in x_first_end) and height != 1:
+            near[1] |= 1 << tile
+        if height < 2 and not (across and ((2, 3)[height], second) in x_first_middle):
+            far[1] |= 1 << tile
+    return near, far
+
 
 def words_of(plan):
     codes = list(plan)
@@ -86,6 +106,20 @@
 
 def layer_kernel(
     sp_count,
+    stream_hbm,
+    pre_hbm,
+    value_hbm,
+    post_hbm,
+    taps_hbm,
+    ids_hbm,
+    weight_hbm,
+    gain_hbm,
+    post_gain_hbm,
+    out_hbm,
+    gate_hbm,
+    up_hbm,
+    down_hbm,
+    result_ref,
     stream_ref,
     pre_ref,
     value_ref,
@@ -95,11 +129,6 @@
     weight_ref,
     gain_ref,
     post_gain_ref,
-    out_hbm,
-    gate_hbm,
-    up_hbm,
-    down_hbm,
-    result_ref,
     out_w,
     gate_w,
     up_w,
@@ -174,14 +203,31 @@
             device_id_type=pl.DeviceIdType.MESH,
         )
 
-    loads = [
-        pltpu.make_async_copy(source, target, load_sem.at[i])
-        for i, (source, target) in enumerate(
-            ((out_hbm, out_w), (gate_hbm.at[0], gate_w), (up_hbm.at[0], up_w), (down_hbm.at[0], down_w))
-        )
-    ]
-    for load in loads:
+    sources = dict(
+        pre=(pre_hbm, pre_ref),
+        value=(value_hbm, value_ref),
+        ids=(ids_hbm, ids_ref),
+        weight=(weight_hbm, weight_ref),
+        taps=(taps_hbm, taps_ref),
+        post=(post_hbm, post_ref),
+        out=(out_hbm, out_w),
+        stream=(stream_hbm, stream_ref),
+        gain=(gain_hbm, gain_ref),
+        gate=(gate_hbm.at[0], gate_w),
+        up=(up_hbm.at[0], up_w),
+        down=(down_hbm.at[0], down_w),
+        post_gain=(post_gain_hbm, post_gain_ref),
+    )
+    loads = {
+        name: pltpu.make_async_copy(source, target, load_sem.at[i])
+        for i, (name, (source, target)) in enumerate(sources.items())
+    }
+    for load in loads.values():
         load.start()
+
+    def loaded(*wanted):
+        for name in wanted:
+            loads[name].wait()
 
     barrier = pltpu.get_barrier_semaphore()
 
@@ -200,6 +246,7 @@
         met = met + jnp.where(there, 1, 0)
     pl.semaphore_wait(barrier, met)
 
+    loaded("pre", "value")
     gated = (pre_ref[...].astype(f32) * value_ref[...].astype(f32)).astype(bf16)
     tail[...] = gated[seq - 16 :]
     rim_copy = remote(tail, rim, rim_sem.at[0], rim_sem.at[1], at(sp + 1, tp))
@@ -208,6 +255,7 @@
     def _():
         rim_copy.start()
 
+    loaded("ids", "weight")
     expert = lax.broadcasted_iota(jnp.int32, (sp_count, seq), 0)
     spread = jnp.zeros((sp_count, seq), f32)
     for k in range(ids_ref.shape[0]):
@@ -235,6 +283,7 @@
     send_scales(sp)
     padded[8:, :] = gated.astype(f32)
     padded[:8, :] = jnp.zeros((8, padded.shape[1]), f32)
+    loaded("taps", "post")
     tap_count = taps_ref.shape[0]
     taps = taps_ref[...].astype(f32)
 
@@ -246,7 +295,7 @@
         mixed[:count, :] = (post_ref[:count, :].astype(f32) * convolved).astype(bf16)
 
     mix(seq)
-    loads[0].wait()
+    loaded("out")
 
     def rows_of(core):
         return jnp.concatenate(
@@ -312,6 +361,7 @@
         pair_copy(i).wait_recv()
     send_y(PIECES - 1)
     pair_copy(1).wait_recv()
+    loaded("stream", "gain")
 
     def height_of(relative):
         inner = jnp.where(relative == 0, 0, jnp.where(relative == 1, -1, relative - 1))
@@ -357,8 +407,7 @@
         pass_on(2, sp, y, p).start()
         pass_on(3, sp, y, p).start()
 
-    for load in loads[1:]:
-        load.wait()
+    loaded("gate", "up", "down")
 
     def wait_piece(group, yy, p):
         pass_on(2, group, yy, p).wait_recv()
@@ -445,24 +494,27 @@
         share(0, group, yy).wait_recv()
         share(2, group, yy).start()
 
-    def chain_copy(group, yy):
+    def own_half(yy, h):
+        return pl.ds(pl.multiple_of(yy * half + h * rows, rows), rows)
+
+    def chain_copy(group, yy, h):
         rising = lax.div(group, 2) > z
         return remote(
-            part.at[group, tile_rows(yy), :],
-            chain_in.at[jnp.where(rising, 0, 1), group, tile_rows(yy), :],
+            part.at[group, own_half(yy, h), :],
+            chain_in.at[jnp.where(at_end, 0, 1), group, own_half(yy, h), :],
             chain_send.at[0],
-            chain_recv.at[group, yy],
+            chain_recv.at[group, yy, h],
             at(sp + jnp.where(rising, 2, -2), tp),
         )
 
-    def wait_chain(sides, group, yy):
-        tiles = chain_in.at[pl.ds(0, sides), group, tile_rows(yy), :]
-        remote(tiles, tiles, chain_send.at[0], chain_recv.at[group, yy], at(sp, sibling)).wait_recv()
+    def wait_chain(sides, group, yy, h):
+        tiles = chain_in.at[pl.ds(0, sides), group, own_half(yy, h), :]
+        remote(tiles, tiles, chain_send.at[0], chain_recv.at[group, yy, h], at(sp, sibling)).wait_recv()
 
     diagonal = lax.broadcasted_iota(jnp.int32, (half, half), 0) == lax.broadcasted_iota(jnp.int32, (half, half), 1)
 
     def project_down(tile):
-        height, group, yy = tile_at(tile)
+        _, group, yy = tile_at(tile)
         both = hidden.at[group, pl.ds(0, 2), tile_rows(yy), :]
         remote(both, both, hid_send.at[1], mate_hid_recv.at[group, yy], at(sp, sibling)).wait_recv()
         own_rows = tile_rows(yy)
@@ -477,13 +529,14 @@
         weight = jnp.sum(jnp.where(diagonal, weight, 0.0), axis=1, keepdims=True)
         part[group, own_rows, :] = (out.astype(bf16).astype(f32) * weight).astype(bf16)
 
-        @pl.when(((height > z) & (z == 0)) | ((height < z) & (z == last)))
-        def _():
-            chain_copy(group, yy).start()
-
-    def x_copy(group, yy):
+    def x_copy(group, yy, h):
+        height = lax.div(group, 2)
         return remote(
-            part.at[group, tile_rows(yy), :], x_in.at[tile_rows(yy), :], x_send.at[0], x_recv.at[yy], at(across, tp)
+            part.at[group, own_half(yy, h), :],
+            x_in.at[height, own_half(yy, h), :],
+            x_send.at[0],
+            x_recv.at[height, yy, h],
+            at(across, tp),
         )
 
     def hand_over(to):
@@ -491,45 +544,56 @@
             final.at[pl.ds(to * rows, rows), :], columns.at[tp], fin_send.at[0], fin_recv.at[tp], at(sp, to)
         )
 
-    def toward_home(tile):
+    def flag(words, position):
+        return lax.rem(lax.shift_right_logical(jnp.where(at_end, words[0], words[1]), position), 2)
+
+    x_first_words = [sum(1 << (2 * height + second) for height, second in chosen) for chosen in x_first]
+    near_words, far_words = comes_along_z(*x_first)
+
+    def toward_home(code):
+        tile, h = lax.div(code, 2), lax.rem(code, 2)
+        relative, second = lax.div(tile, 4), lax.rem(tile, 2)
         height, group, yy = tile_at(tile)
-        own_rows = tile_rows(yy)
+        own_rows = own_half(yy, h)
+        own_side = lax.rem(lax.div(tile, 2), 2) == 0
+        over_x = (relative == 0) | (flag(x_first_words, 2 * relative + second) == 1)
+        near, far = flag(near_words, tile), flag(far_words, tile)
         total[...] = part[group, own_rows, :].astype(f32)
-        both_sides = (height == z) & jnp.logical_not(at_end)
-
-        @pl.when(both_sides)
-        def _():
-            wait_chain(2, group, yy)
-
-        @pl.when(jnp.logical_not(both_sides))
-        def _():
-            wait_chain(1, group, yy)
-
-        for side, comes in enumerate(((height >= z) & (z > 0), (height <= z) & (z < last))):
-
-            @pl.when(comes)
+        for count in (1, 2):
+
+            @pl.when(near + far == count)
+            def _():
+                wait_chain(count, group, yy, h)
+
+        for side, comes in enumerate((near, far)):
+
+            @pl.when(comes == 1)
             def _():
                 total[...] = total[...] + chain_in[side, group, own_rows, :].astype(f32)
 
+        @pl.when(own_side & over_x)
+        def _():
+            x_copy(group, yy, h).wait_recv()
+            total[...] = total[...] + x_in[height, own_rows, :].astype(f32)
+
         @pl.when(group != sp)
         def _():
             part[group, own_rows, :] = total[...].astype(bf16)
 
-            @pl.when(height != z)
+            @pl.when(own_side | jnp.logical_not(over_x))
             def _():
-                chain_copy(group, yy).start()
-
-            @pl.when(height == z)
+                chain_copy(group, yy, h).start()
+
+            @pl.when(jnp.logical_not(own_side) & over_x)
             def _():
-                x_copy(group, yy).start()
+                x_copy(group, yy, h).start()
 
         @pl.when(group == sp)
         def _():
-            x_copy(group, yy).wait_recv()
-            final[own_rows, :] = (total[...] + x_in[own_rows, :].astype(f32)).astype(bf16)
+            final[own_rows, :] = total[...].astype(bf16)
             for to in range(4):
 
-                @pl.when((tp != to) & (yy == to // 2))
+                @pl.when((tp != to) & (2 * yy + h == to))
                 def _():
                     hand_over(to).start()
 
@@ -560,6 +624,7 @@
         remote(
             final.at[pl.ds(0, rows), :], columns.at[whose], fin_send.at[0], fin_recv.at[whose], at(sp, sibling)
         ).wait_recv()
+    loaded("post_gain")
     combined = jnp.concatenate([columns[k] for k in range(4)], 1).astype(f32)
     result_ref[...] = (
         resid[...].astype(f32) + scaled_norm(combined, post_gain_ref[...].reshape(1, width))
@@ -592,9 +657,17 @@
         tiles = hidden.at[:, 0]
         receive = mate_hid_recv.at[0, 0] if way else hid_recv.at[0, 0]
         remote(tiles, tiles, hid_send.at[way], receive, at(sp, sibling)).wait_send()
-    chained = part.at[pl.ds(0, sp_count - 2)]
-    remote(chained, chained, chain_send.at[0], chain_recv.at[0, 0], at(sp, sibling)).wait_send()
-    remote(part.at[0], x_in, x_send.at[0], x_recv.at[0], at(across, tp)).wait_send()
+    for chosen, its in zip(x_first, (at_end, jnp.logical_not(at_end))):
+
+        @pl.when(its)
+        def _():
+            crossed = part.at[pl.ds(0, len(chosen) + 2), pl.ds(0, half), :]
+            remote(crossed, crossed, x_send.at[0], x_recv.at[0, 0, 0], at(across, tp)).wait_send()
+            rising = 2 * (sp_count - 2) - len(chosen)
+            across_count = 1 if rising <= sp_count else 2 if rising % 2 == 0 else 3
+            chained = hidden.at[pl.ds(0, rising // across_count), pl.ds(0, across_count), pl.ds(0, half), :]
+            remote(chained, chained, chain_send.at[0], chain_recv.at[0, 0, 0], at(sp, sibling)).wait_send()
+
     handed = final.at[pl.ds(0, 3 * rows), :]
     remote(handed, handed, fin_send.at[0], fin_recv.at[0], at(sp, sibling)).wait_send()
 
@@ -621,7 +694,10 @@
     cols = down_proj.shape[2]
     bf16, f32 = jnp.bfloat16, jnp.float32
     dma = pltpu.SemaphoreType.DMA
-    scratch = [
+    small = (
+        stream_in, pre_gate, value_in, post_gate, conv_taps, route_ids.T, route_weight.T, ffn_gain, post_gain
+    )
+    scratch = [pltpu.VMEM(array.shape, array.dtype) for array in small] + [
         pltpu.VMEM(out_weight.shape, bf16),
         pltpu.VMEM(gate_proj.shape[1:], bf16),
         pltpu.VMEM(up_proj.shape[1:], bf16),
@@ -641,11 +717,11 @@
         pltpu.VMEM((sp_count, 4, seq, units), bf16),
         pltpu.VMEM((sp_count, seq, cols), bf16),
         pltpu.VMEM((2, sp_count, seq, cols), bf16),
-        pltpu.VMEM((seq, cols), bf16),
-        pltpu.VMEM((2 * rows, cols), f32),
+        pltpu.VMEM((sp_count // 2, seq, cols), bf16),
+        pltpu.VMEM((rows, cols), f32),
         pltpu.VMEM((seq, cols), bf16),
         pltpu.VMEM((4, rows, cols), bf16),
-        dma((4,)),
+        dma((13,)),
         dma((2,)),
         dma((1,)),
         dma((4,)),
@@ -660,9 +736,9 @@
         dma((sp_count, 2)),
         dma((sp_count, 2)),
         dma((1,)),
-        dma((sp_count, 2)),
+        dma((sp_count, 2, 2)),
         dma((1,)),
-        dma((2,)),
+        dma((sp_count // 2, 2, 2)),
         dma((1,)),
         dma((4,)),
     ]
@@ -671,22 +747,14 @@
     return pl.pallas_call(
         functools.partial(layer_kernel, sp_count),
         out_shape=jax.ShapeDtypeStruct((rows, width), bf16),
-        in_specs=[vmem] * 9 + [anywhere] * 4,
+        in_specs=[anywhere] * 13,
         out_specs=vmem,
         scratch_shapes=scratch,
         compiler_params=pltpu.CompilerParams(
             collective_id=0, has_side_effects=True, vmem_limit_bytes=58 * 1024 * 1024
         ),
     )(
-        stream_in,
-        pre_gate,
-        value_in,
-        post_gate,
-        conv_taps,
-        route_ids.T,
-        route_weight.T,
-        ffn_gain,
-        post_gain,
+        *small,
         out_weight,
         gate_proj,
         up_proj,

time: 82.8 us -> 79.9 us (0.965)
  Pallas kernels: 80.6 us -> 76.9 us
    pallas_call x1, Pallas kernels: 80.6 us -> 76.9 us  [dense_layer(): pl.pallas_call(functools.partial(layer_kernel, sp_count), out_shape=jax.S...]
where the time goes in v4:
time: 79.9 us; the launch traced here: 78.6 us
  Pallas kernels  76.9 us (96%)
  local copies, waits for them, and re-layouts  1.67 us (2%)
    pallas_call x1, Pallas kernels, dense_layer(): pl.pallas_call(functools.partial(layer_kernel, sp_count), out_shape=jax.S...  76.9 us
    unnamed x1, local copies, waits for them, and re-layouts  1.67 us

profile of v4, /device:TPU:9, one launch (start us, length us, event | category | flops | bytes accessed | tf_op | source)
XLA Modules:
  0.0 78.6 jit_solution(15492870876833641306)
XLA Ops:
  0.0 76.9 %shard_map.127 = bf16[64,2048]{1,0:T(8,128)(2,1)} custom-call(bf16[64,2048]{1,0:T(8,128)(2,1)} %stream_hbm.1, bf16[256,256]{1,0:T(8,128)(2,1)} %pre_hbm.1, bf16[256,256]{1,0:T(8,128)(2,1)} %value_hbm.1, bf16[256,256]{1,0:T(8,128)(2,1)} %post_hbm.1, bf16[3,256]{1,0:T(4,128)(2,1)} %taps_hbm.1, s32[4,256]{1,0:T(4,128)} %bitcast.2, f32[4,256]{1,0:T(4,128)} %bitcast.3, ...), custom_call_target="tpu_custom_call" | custom-call | tf_op jit(solution)/shard_map/pallas_call | solution.py:747
  76.9 1.7 %copy.15 = bf16[64,2048]{1,0:T(8,128)(2,1)} copy(bf16[64,2048]{1,0:T(8,128)(2,1)} %shard_map.127) | data formatting | bytes 524288

commit v5 on v4

--- a/solution.py
+++ b/solution.py
@@ -50,28 +50,25 @@
 PIECES = 4
 PLANNED_GROUPS = 8
 end_plan = (
-    8, 96, 10, 5, 11, 9, 4, 7, 100, 16, 6, 18, 19, 97, 42, 41, 17, 40, 43, 102,
-    24, 104, 27, 25, 26, 59, 50, 108, 31, 56, 29, 57, 30, 28, 58, 109, 48, 51, 49, 12,
-    141, 106, 14, 173, 218, 110, 63, 60, 133, 62, 135, 13, 219, 140, 15, 61, 20, 22, 111, 101,
-    172, 216, 165, 139, 129, 23, 21, 45, 217, 44, 143, 66, 65, 175, 105, 52, 47, 54, 35, 137,
-    223, 33, 46, 67, 142, 64, 55, 128, 53, 32, 222, 174, 221, 107, 103, 161, 34, 171, 215, 167,
-    214, 98, 207, 132, 39, 206, 169, 220, 138, 36, 136, 38, 37, 211, 210, 170, 213, 99, 203, 134,
-    212, 168, 166, 204, 202, 205, 209, 131, 163, 199, 164, 198, 130, 208, 200, 201, 162, 197, 160, 195,
-    196, 194, 193, 192,
+    8, 4, 96, 9, 10, 6, 11, 5, 100, 7, 16, 17, 97, 19, 18, 25, 133, 104, 40, 26,
+    27, 102, 129, 24, 108, 28, 48, 29, 128, 135, 106, 31, 30, 13, 109, 56, 141, 110, 32, 12,
+    14, 173, 60, 15, 218, 20, 139, 161, 140, 101, 172, 219, 21, 165, 203, 111, 22, 143, 23, 44,
+    175, 67, 223, 103, 217, 160, 216, 66, 105, 222, 167, 52, 64, 65, 142, 107, 134, 137, 174, 221,
+    171, 215, 98, 220, 166, 136, 214, 36, 204, 207, 206, 169, 99, 138, 205, 132, 168, 210, 170, 213,
+    211, 164, 212, 131, 202, 163, 198, 209, 130, 199, 208, 162, 196, 200, 201, 194, 197, 195, 192, 193,
 )
 middle_plan = (
-    16, 8, 4, 17, 96, 10, 11, 18, 6, 9, 19, 13, 100, 24, 27, 5, 7, 97, 25, 15,
-    26, 14, 29, 12, 35, 34, 108, 42, 40, 31, 41, 30, 101, 28, 68, 133, 128, 70, 129, 69,
-    43, 109, 32, 104, 71, 102, 132, 59, 22, 33, 57, 161, 98, 160, 20, 58, 141, 21, 51, 56,
-    48, 23, 140, 49, 65, 50, 173, 110, 172, 62, 61, 64, 105, 66, 67, 218, 47, 131, 63, 46,
-    44, 60, 143, 45, 111, 219, 106, 103, 175, 54, 55, 53, 52, 165, 217, 135, 216, 164, 142, 223,
-    107, 222, 174, 139, 167, 202, 137, 36, 38, 221, 37, 39, 207, 171, 215, 136, 134, 99, 206, 203,
-    214, 166, 163, 220, 199, 138, 198, 205, 168, 170, 200, 169, 211, 213, 212, 210, 204, 130, 162, 201,
-    197, 196, 209, 194, 208, 195, 193, 192,
+    8, 17, 9, 16, 96, 18, 10, 11, 19, 5, 100, 25, 12, 26, 104, 6, 13, 27, 4, 7,
+    24, 14, 15, 97, 28, 29, 101, 40, 137, 31, 30, 102, 69, 68, 133, 70, 71, 108, 109, 56,
+    32, 20, 48, 22, 110, 44, 141, 21, 23, 103, 66, 105, 60, 140, 111, 67, 143, 132, 64, 172,
+    128, 129, 173, 134, 136, 106, 65, 175, 135, 218, 165, 52, 164, 167, 142, 223, 107, 166, 222, 174,
+    139, 219, 98, 207, 171, 202, 221, 36, 215, 214, 206, 169, 205, 204, 220, 138, 99, 170, 217, 213,
+    212, 131, 203, 160, 216, 210, 163, 168, 198, 211, 130, 201, 199, 161, 162, 200, 197, 209, 194, 196,
+    208, 195, 193, 192,
 )
 x_first = (
-    ((1, 0), (1, 1), (2, 0),),
-    ((2, 0), (2, 1),),
+    ((1, 0), (2, 0), (2, 1),),
+    ((2, 0), (3, 0),),
 )
 
 def comes_along_z(x_first_end, x_first_middle):
@@ -162,6 +159,7 @@
     scale_recv,
     tok_send,
     tok_recv,
+    across_recv,
     mate_recv,
     hid_send,
     hid_recv,
@@ -378,7 +376,13 @@
 
     def pass_on(way, group, yy, p):
         piece = piece_of(group, yy, p)
-        receive = mate_recv.at[group, yy] if way == 3 else tok_recv.at[group, yy, p]
+        height = lax.div(group, 2)
+        if way == 2:
+            receive = across_recv.at[height, yy]
+        elif way == 3:
+            receive = mate_recv.at[group, yy]
+        else:
+            receive = tok_recv.at[height, yy, p]
         return remote(piece, piece, tok_send.at[way], receive, devices[way])
 
     def sent(way, group_count, row_count):
@@ -410,7 +414,7 @@
     loaded("gate", "up", "down")
 
     def wait_piece(group, yy, p):
-        pass_on(2, group, yy, p).wait_recv()
+        pass_on(0, group, yy, p).wait_recv()
 
     def wait_mate(group, yy):
         block = block_of(group, yy, 1 - c)
@@ -442,15 +446,16 @@
             pass_on(2, group, yy, p).start()
 
     def take_across(code):
-        _, height, yy, p = block_at(code)
+        _, height, yy, _ = block_at(code)
         group = 2 * height + 1 - x
 
         @pl.when(lax.rem(code, 2 * PIECES) == 0)
         def _():
             wait_scales(group)
 
-        wait_piece(group, yy, p)
-        pass_on(3, group, yy, p).start()
+        block = block_of(group, yy, c)
+        remote(block, block, tok_send.at[2], across_recv.at[height, yy], devices[2]).wait_recv()
+        remote(block, block, tok_send.at[3], mate_recv.at[group, yy], devices[3]).start()
 
     def pass_held(code):
         p = lax.rem(code, PIECES)
@@ -730,7 +735,8 @@
         dma((3,)),
         dma((sp_count,)),
         dma((5,)),
-        dma((sp_count, 2, PIECES)),
+        dma((sp_count // 2, 2, PIECES)),
+        dma((sp_count // 2, 2)),
         dma((sp_count, 2)),
         dma((3,)),
         dma((sp_count, 2)),

time: 79.9 us -> 78.1 us (0.977); the launches traced: 78.6 us -> 77.8 us
  Pallas kernels: 76.9 us -> 76.1 us
where the time goes in v5:
time: 78.1 us; the launch traced here: 77.8 us
  Pallas kernels  76.1 us (97%)
  local copies, waits for them, and re-layouts  1.67 us (2%)
    pallas_call x1, Pallas kernels, dense_layer(): pl.pallas_call(functools.partial(layer_kernel, sp_count), out_shape=jax.S...  76.1 us
    unnamed x1, local copies, waits for them, and re-layouts  1.67 us

profile of v5, /device:TPU:9, one launch (start us, length us, event | category | flops | bytes accessed | tf_op | source)
XLA Modules:
  0.0 77.8 jit_solution(16604737710773303470)
XLA Ops:
  0.0 76.1 %shard_map.127 = bf16[64,2048]{1,0:T(8,128)(2,1)} custom-call(bf16[64,2048]{1,0:T(8,128)(2,1)} %stream_hbm.1, bf16[256,256]{1,0:T(8,128)(2,1)} %pre_hbm.1, bf16[256,256]{1,0:T(8,128)(2,1)} %value_hbm.1, bf16[256,256]{1,0:T(8,128)(2,1)} %post_hbm.1, bf16[3,256]{1,0:T(4,128)(2,1)} %taps_hbm.1, s32[4,256]{1,0:T(4,128)} %bitcast.2, f32[4,256]{1,0:T(4,128)} %bitcast.3, ...), custom_call_target="tpu_custom_call" | custom-call | tf_op jit(solution)/shard_map/pallas_call | solution.py:753
  76.2 1.7 %copy.15 = bf16[64,2048]{1,0:T(8,128)(2,1)} copy(bf16[64,2048]{1,0:T(8,128)(2,1)} %shard_map.127) | data formatting | bytes 524288

commit v6 on v5

--- a/solution.py
+++ b/solution.py
@@ -50,25 +50,25 @@
 PIECES = 4
 PLANNED_GROUPS = 8
 end_plan = (
-    8, 4, 96, 9, 10, 6, 11, 5, 100, 7, 16, 17, 97, 19, 18, 25, 133, 104, 40, 26,
-    27, 102, 129, 24, 108, 28, 48, 29, 128, 135, 106, 31, 30, 13, 109, 56, 141, 110, 32, 12,
-    14, 173, 60, 15, 218, 20, 139, 161, 140, 101, 172, 219, 21, 165, 203, 111, 22, 143, 23, 44,
-    175, 67, 223, 103, 217, 160, 216, 66, 105, 222, 167, 52, 64, 65, 142, 107, 134, 137, 174, 221,
-    171, 215, 98, 220, 166, 136, 214, 36, 204, 207, 206, 169, 99, 138, 205, 132, 168, 210, 170, 213,
-    211, 164, 212, 131, 202, 163, 198, 209, 130, 199, 208, 162, 196, 200, 201, 194, 197, 195, 192, 193,
+    4, 8, 10, 96, 9, 11, 5, 100, 6, 7, 17, 18, 97, 40, 19, 25, 102, 16, 24, 27,
+    104, 128, 26, 48, 108, 28, 129, 29, 106, 161, 56, 31, 30, 133, 109, 141, 13, 110, 173, 137,
+    14, 219, 218, 32, 15, 12, 135, 60, 101, 140, 20, 165, 172, 202, 22, 111, 143, 216, 217, 23,
+    21, 66, 44, 64, 67, 65, 175, 223, 222, 103, 203, 105, 142, 167, 207, 52, 174, 221, 139, 107,
+    220, 134, 169, 171, 214, 98, 160, 206, 136, 36, 215, 166, 168, 205, 138, 210, 99, 170, 213, 211,
+    131, 212, 132, 204, 163, 198, 209, 130, 199, 208, 162, 196, 164, 197, 201, 200, 194, 195, 192, 193,
 )
 middle_plan = (
-    8, 17, 9, 16, 96, 18, 10, 11, 19, 5, 100, 25, 12, 26, 104, 6, 13, 27, 4, 7,
-    24, 14, 15, 97, 28, 29, 101, 40, 137, 31, 30, 102, 69, 68, 133, 70, 71, 108, 109, 56,
-    32, 20, 48, 22, 110, 44, 141, 21, 23, 103, 66, 105, 60, 140, 111, 67, 143, 132, 64, 172,
-    128, 129, 173, 134, 136, 106, 65, 175, 135, 218, 165, 52, 164, 167, 142, 223, 107, 166, 222, 174,
-    139, 219, 98, 207, 171, 202, 221, 36, 215, 214, 206, 169, 205, 204, 220, 138, 99, 170, 217, 213,
-    212, 131, 203, 160, 216, 210, 163, 168, 198, 211, 130, 201, 199, 161, 162, 200, 197, 209, 194, 196,
+    9, 8, 17, 96, 4, 18, 19, 6, 11, 10, 16, 25, 100, 7, 24, 5, 32, 13, 12, 104,
+    27, 15, 14, 26, 108, 28, 29, 31, 101, 30, 71, 69, 70, 40, 68, 102, 109, 97, 20, 48,
+    22, 21, 44, 23, 56, 103, 141, 140, 110, 129, 133, 132, 64, 65, 66, 173, 105, 135, 128, 67,
+    219, 172, 60, 134, 111, 106, 164, 218, 143, 166, 204, 137, 165, 175, 203, 52, 205, 136, 222, 223,
+    167, 107, 142, 98, 206, 139, 174, 221, 161, 36, 207, 171, 214, 215, 220, 138, 99, 169, 170, 217,
+    213, 160, 212, 131, 168, 216, 202, 163, 198, 210, 211, 130, 201, 199, 162, 197, 200, 209, 196, 194,
     208, 195, 193, 192,
 )
 x_first = (
-    ((1, 0), (2, 0), (2, 1),),
-    ((2, 0), (3, 0),),
+    ((2, 0), (2, 1),),
+    ((1, 0), (2, 0), (3, 0),),
 )
 
 def comes_along_z(x_first_end, x_first_middle):
@@ -253,13 +253,6 @@
     def _():
         rim_copy.start()
 
-    loaded("ids", "weight")
-    expert = lax.broadcasted_iota(jnp.int32, (sp_count, seq), 0)
-    spread = jnp.zeros((sp_count, seq), f32)
-    for k in range(ids_ref.shape[0]):
-        spread = spread + jnp.where(expert == ids_ref[k : k + 1, :], weight_ref[k : k + 1, :], 0.0)
-    scales[sp] = spread
-
     routes = (
         lambda group: (lax.div(group, 2) <= z) & (z < last),
         lambda group: (lax.div(group, 2) >= z) & (z > 0),
@@ -278,7 +271,6 @@
 
         scale_copy(2, group).start()
 
-    send_scales(sp)
     padded[8:, :] = gated.astype(f32)
     padded[:8, :] = jnp.zeros((8, padded.shape[1]), f32)
     loaded("taps", "post")
@@ -337,6 +329,15 @@
     pair_copy(0).wait_recv()
     for p in range(PIECES - 1):
         send_y(p)
+
+    loaded("ids", "weight")
+    expert = lax.broadcasted_iota(jnp.int32, (sp_count, seq), 0)
+    spread = jnp.zeros((sp_count, seq), f32)
+    for k in range(ids_ref.shape[0]):
+        spread = spread + jnp.where(expert == ids_ref[k : k + 1, :], weight_ref[k : k + 1, :], 0.0)
+    scales[sp] = spread
+
+    send_scales(sp)
 
     @pl.when(sp > 0)
     def _():

time: 78.1 us -> 77.8 us (level)
  no operation moved by 1% of the time
where the time goes in v6:
time: 77.8 us; the launch traced here: 77.7 us
  Pallas kernels  76 us (98%)
  local copies, waits for them, and re-layouts  1.67 us (2%)
    pallas_call x1, Pallas kernels, dense_layer(): pl.pallas_call(functools.partial(layer_kernel, sp_count), out_shape=jax.S...  76 us
    unnamed x1, local copies, waits for them, and re-layouts  1.67 us

profile of v6, /device:TPU:9, one launch (start us, length us, event | category | flops | bytes accessed | tf_op | source)
XLA Modules:
  0.0 77.7 jit_solution(8076308560458608175)
XLA Ops:
  0.0 76.0 %shard_map.127 = bf16[64,2048]{1,0:T(8,128)(2,1)} custom-call(bf16[64,2048]{1,0:T(8,128)(2,1)} %stream_hbm.1, bf16[256,256]{1,0:T(8,128)(2,1)} %pre_hbm.1, bf16[256,256]{1,0:T(8,128)(2,1)} %value_hbm.1, bf16[256,256]{1,0:T(8,128)(2,1)} %post_hbm.1, bf16[3,256]{1,0:T(4,128)(2,1)} %taps_hbm.1, s32[4,256]{1,0:T(4,128)} %bitcast.2, f32[4,256]{1,0:T(4,128)} %bitcast.3, ...), custom_call_target="tpu_custom_call" | custom-call | tf_op jit(solution)/shard_map/pallas_call | solution.py:754
  76.0 1.7 %copy.15 = bf16[64,2048]{1,0:T(8,128)(2,1)} copy(bf16[64,2048]{1,0:T(8,128)(2,1)} %shard_map.127) | data formatting | bytes 524288
